TPU v7x, 256 devices: a whole 4x4x8 slice. The times are simulated.
256 devices in a mesh: gr: 2 (over z_hi), sp: 16 (over z_lo, x), tp: 8 (over y, core).
Axes of the slice: x: 4, y: 4, z: 8 (z_hi: 2, z_lo: 4; z = z_hi * 4 + z_lo), core: 2. Of those that a mesh axis runs over, the one named last changes fastest.
Arguments:
- tokens: bfloat16 [8, 65536, 2048], P('gr', ('sp', 'tp')), parts along dimension 0, may hold values from -6 to 6
- norm_gain: float32 [2048], replicated, may hold values from 0.1 to 1.9
- w_key: bfloat16 [2048, 256], replicated, may hold values from -0.125 to 0.125
- w_value: bfloat16 [2048, 256], replicated, may hold values from -0.125 to 0.125
- new_query: bfloat16 [8, 32, 64], P('gr'), parts along dimension 0, may hold values from -360 to 360
- cum_gate: float32 [32, 8, 8192], P(('gr', 'sp'), 'tp'), parts along dimension 0, may hold values from -8193 to 0, as said below
Outputs:
- kv_cache: bfloat16 [32, 8, 8192, 128], P(('gr', 'sp'), 'tp'), parts along dimension 0
- first_read: float32 [8, 32, 64], P('gr'), parts along dimension 0
There are 2 independent parts, one for each index of `gr`. A program takes and returns all parts, laid end to end along the dimension named above; an argument that names none is the same for every part. Nothing has to cross between parts.
Inputs may be any that keep to these rules, and one draw needn't show every extreme that they name: `cum_gate`: for each sequence and key head, the running sum along the positions of the sequence of negative log forget gates; it never rises from one position to the next.
All inputs are finite; a program needn't handle non-finite values.
Results may differ from a plain program's by a relative error of at most 0.0014.
The roundings to bfloat16 on the way count: a program that leaves them out, or rounds other values in their place, can miss the bound.
Values may be sent and summed in bfloat16 or wider, within the bound.
A program may use at most 64 MiB of HBM per device.

v0:
```python
import jax
import jax.numpy as jnp
from jax import lax
from jax.sharding import Mesh
from jax.sharding import PartitionSpec as P

HD = 64
SP = ("sp_0", "sp_1")
TP = ("tp_0", "tp_1")
SP_TP = ("sp_0", "sp_1", "tp_0", "tp_1")
GR_SP = ("gr", "sp_0", "sp_1")


NORM_FLOOR = 0.05
SCORE_FLOOR = -1e30


def collected_together(array, axis):
    leaves = jax.tree.leaves(array)
    order = sorted(range(len(leaves)), key=lambda k: -leaves[k].size)
    width = (1, *leaves[order[0]].shape)[-1]
    lines = [
        jnp.pad(leaves[k].reshape(-1), (0, -leaves[k].size % width)).reshape(-1, width)
        for k in order
    ]
    both, at, found = (lax.all_gather(jnp.concatenate(lines), axis), 0, {})
    for k, line in zip(order, lines):
        slab = both[:, at : at + len(line)].reshape(len(both), -1)
        found[k] = slab[:, : leaves[k].size].reshape(-1, *leaves[k].shape)
        at += len(line)
    numbers = iter(range(len(leaves)))
    return jax.tree.map(lambda _: found[next(numbers)], array)


def merged_by_axis(array, axes, combine):
    for axis in axes:
        pieces = collected_together(array, axis)
        array = jax.tree.map(lambda part: part[0], pieces)
        for k in range(1, lax.axis_size(axis)):
            array = combine(array, jax.tree.map(lambda part: part[k], pieces))
    return array


def combine(left_side, right_side):
    out_left, top_left, sum_left = left_side
    out_right, top_right, sum_right = right_side
    merged_top = jnp.maximum(top_left, top_right)
    factor_left = jnp.exp(top_left - merged_top)
    factor_right = jnp.exp(top_right - merged_top)
    merged_out = out_left * factor_left[..., None] + out_right * factor_right[..., None]
    merged_sum = sum_left * factor_left + sum_right * factor_right
    return (merged_out, merged_top, merged_sum)


def shards(tokens, norm_gain, w_key, w_value, new_query, cum_gate):
    seq_count, positions, model_width = tokens.shape
    sp_count = lax.axis_size(SP)
    tp_count = lax.axis_size(TP)
    kv_heads = w_key.shape[1] // HD
    classes = sp_count // seq_count
    halves = tp_count // kv_heads
    piece_len = positions // (classes * halves)
    widened = tokens.astype(jnp.float32)
    inverse_rms = lax.rsqrt(jnp.mean(widened * widened, axis=-1, keepdims=True) + NORM_FLOOR)
    normed = (widened * inverse_rms * norm_gain).astype(jnp.bfloat16)
    shaped = normed.reshape(seq_count, classes, halves, piece_len, model_width)
    key_heads = w_key.reshape(model_width, kv_heads, HD)
    value_heads = w_value.reshape(model_width, kv_heads, HD)
    keys_made = jnp.einsum(
        "gcbkd,dhe->gchbke", shaped, key_heads, preferred_element_type=jnp.float32
    ).astype(jnp.bfloat16)
    values_made = jnp.einsum(
        "gcbkd,dhe->gchbke", shaped, value_heads, preferred_element_type=jnp.float32
    ).astype(jnp.bfloat16)
    stacked = jnp.concatenate([keys_made, values_made], axis=-1)
    arrived = lax.all_to_all(
        stacked.reshape(sp_count * tp_count, 1, piece_len, 2 * HD),
        SP_TP,
        split_axis=0,
        concat_axis=1,
        tiled=True,
    )
    kv_cache = arrived.reshape(1, 1, sp_count * tp_count * piece_len, 2 * HD)
    query_heads = new_query.shape[1]
    group_size = query_heads // kv_heads
    seq_index = lax.axis_index(SP) // classes
    head_index = lax.axis_index(TP) // halves
    queries = lax.dynamic_slice(
        new_query, (seq_index, head_index * group_size, 0), (1, group_size, HD)
    )[0]
    keys_here = kv_cache[0, 0, :, :HD]
    values_here = kv_cache[0, 0, :, HD:]
    scores = lax.dot_general(
        queries, keys_here, (((1,), (1,)), ((), ())), preferred_element_type=jnp.float32
    )
    scores = scores * HD ** (-0.5) - cum_gate[0, 0][None, :]
    row_top = jnp.max(scores, axis=1)
    weights = jnp.exp(scores - row_top[:, None])
    row_total = jnp.sum(weights, axis=1)
    summed = jnp.dot(weights, values_here.astype(jnp.float32), precision=lax.Precision.HIGHEST)
    out_full = lax.dynamic_update_slice(
        jnp.zeros((seq_count, query_heads, HD), jnp.float32),
        summed[None],
        (seq_index, head_index * group_size, 0),
    )
    top_full = lax.dynamic_update_slice(
        jnp.full((seq_count, query_heads), SCORE_FLOOR, jnp.float32),
        row_top[None],
        (seq_index, head_index * group_size),
    )
    sum_full = lax.dynamic_update_slice(
        jnp.zeros((seq_count, query_heads), jnp.float32),
        row_total[None],
        (seq_index, head_index * group_size),
    )
    merged_out, merged_top, merged_sum = merged_by_axis(
        (out_full, top_full, sum_full), SP_TP, combine
    )
    first_read = merged_out / merged_sum[..., None]
    return (kv_cache, first_read)


def solution(mesh):
    split = Mesh(
        mesh.devices.reshape(mesh.shape["gr"], 4, 4, 4, 2), ("gr", "sp_0", "sp_1", "tp_0", "tp_1")
    )
    return jax.shard_map(
        shards,
        mesh=split,
        in_specs=(P("gr", SP_TP, None), P(), P(), P(), P("gr", None, None), P(GR_SP, TP, None)),
        out_specs=(P(GR_SP, TP, None, None), P("gr", None, None)),
        check_vma=False,
    )
```

profile of v0, /device:TPU:1, one launch (start us, length us, event | category | flops | bytes accessed | tf_op | source)
XLA Modules:
  0.0 148.2 jit_solution(16346129064091075156)
XLA Ops:
  0.7 5.2 %fusion = f32[4,512]{1,0:T(4,128)S(1)} fusion(bf16[4,512,2048]{2,1,0:T(8,128)(2,1)} %param.6), kind=kLoop, calls=%fused_computation.2 | loop fusion | flops 12580864 | bytes 8396800 | tf_op jit(solution)/shard_map/reduce_sum | solution.py:64
  5.9 0.6 copy.69
  6.6 0.6 copy.68
  7.3 8.6 %fusion.2 = bf16[4,512,2048]{2,1,0:T(8,128)(2,1)} fusion(bf16[4,512,2048]{2,1,0:T(8,128)(2,1)} %param.6, f32[2048]{0:T(1024)S(1)} %copy-done.5, f32[4,512]{1,0:T(4,128)S(1)} %add_rsqrt_fusion), kind=kLoop, calls=%fused_computation.4 | loop fusion | flops 16777216 | bytes 16793600 | tf_op jit(solution)/shard_map/convert_element_type | solution.py:65
  15.8 7.1 %convert_bitcast_fusion = bf16[4,4,4,2,64,64]{5,4,2,3,1,0:T(8,128)(2,1)S(1)} fusion(bf16[4,4,2,64,2048,1]{4,3,5,2,1,0:T(8,128)(2,1)} %bitcast.395, bf16[2048,4,64,1,1,1]{0,2,1,5,4,3:T(8,128)(2,1)S(1)} %bitcast.399), kind=kOutput, calls=%fused_computation.11 | convolution fusion | flops 2148007936 | bytes 10485760 | tf_op jit(solution)/shard_map/gcbkd,dhe->gchbke/dot_general | solution.py:72
  22.9 4.7 %convert_bitcast_fusion.1 = bf16[4,4,4,2,64,64]{5,4,2,3,1,0:T(8,128)(2,1)S(1)} fusion(bf16[4,4,2,64,2048,1]{4,3,5,2,1,0:T(8,128)(2,1)S(1)} %bitcast.396, bf16[2048,4,64,1,1,1]{0,2,1,5,4,3:T(8,128)(2,1)S(1)} %bitcast.398), kind=kOutput, calls=%fused_computation.12 | convolution fusion | flops 2148007936 | bytes 10485760 | tf_op jit(solution)/shard_map/gcbkd,dhe->gchbke/dot_general | solution.py:69
  27.7 1.2 pad_maximum_fusion
  28.9 1.6 %copy.70 = bf16[4,4,4,2,64,128]{5,4,3,2,1,0:T(8,128)(2,1)} copy(bf16[4,4,4,2,64,128]{5,4,2,3,1,0:T(8,128)(2,1)S(1)} %pad_maximum_fusion) | data formatting | bytes 4194304 | tf_op jit(solution)/shard_map/concatenate | solution.py:75
  30.4 13.8 %all-to-all-start = ((bf16[128,1,64,128]{3,2,1,0:T(8,128)(2,1)}), bf16[128,1,64,128]{3,2,1,0:T(8,128)(2,1)S(1)}, u32[]{:S(2)}, u32[]{:S(2)}) async-start(bf16[128,1,64,128]{3,2,1,0:T(8,128)(2,1)} %bitcast.397), calls=%async_computation | async-start | bytes 4194304 | tf_op jit(solution)/shard_map/all_to_all | solution.py:76
  44.3 51.9 %all-to-all-done = bf16[128,1,64,128]{3,2,1,0:T(8,128)(2,1)S(1)} async-done(((bf16[128,1,64,128]{3,2,1,0:T(8,128)(2,1)}), bf16[128,1,64,128]{3,2,1,0:T(8,128)(2,1)S(1)}, u32[]{:S(2)}, u32[]{:S(2)}) %all-to-all-start) | async-done | bytes 2097184 | tf_op jit(solution)/shard_map/all_to_all | solution.py:76
  96.2 0.8 fusion.87
  96.9 0.3 fusion.7
  97.2 0.2 dynamic_update_slice.11
  97.4 0.1 reshape.552
  97.5 0.1 dynamic_update_slice.10
  97.6 0.1 reshape.551
  97.7 1.3 fusion.6
  99.0 0.1 copy.72
  99.1 11.1 %all-gather.4 = f32[4,132,64]{1,2,0:T(8,128)S(1)} all-gather(f32[1,132,64]{1,2,0:T(8,128)S(1)} %copy.72), channel_id=2, replica_groups=mesh['gr'=2,'sp_0'=4,'sp_1'=4,'tp_0'=4,'tp_1'=2] {'sp_0'}, dimensions={0}, use_global_device_ids=true | all-gather | bytes 168960 | tf_op jit(solution)/shard_map/all_gather | solution.py:26
  110.1 0.1 fusion.84
  110.7 0.1 copy.82
  110.7 0.1 copy.81
  110.8 0.1 squeeze.168
  110.9 0.1 squeeze.163
  111.0 0.1 squeeze.164
  111.1 0.1 squeeze.166
  111.2 0.1 bitcast_maximum_fusion.6
  111.2 0.1 copy.86
  111.3 0.1 copy.85
  111.5 0.1 maximum_bitcast_fusion.1
  111.6 9.4 %all-gather.5 = f32[4,132,64]{1,2,0:T(8,128)S(1)} all-gather(f32[1,132,64]{1,2,0:T(8,128)S(1)} %maximum_bitcast_fusion.1), channel_id=3, replica_groups=mesh['gr'=2,'sp_0'=4,'sp_1'=4,'tp_0'=4,'tp_1'=2] {'sp_1'}, dimensions={0}, use_global_device_ids=true | all-gather | bytes 168960 | tf_op jit(solution)/shard_map/all_gather | solution.py:26
  120.9 0.1 fusion.83
  121.5 0.1 copy.96
  121.5 0.1 copy.95
  121.6 0.1 squeeze.184
  121.7 0.1 squeeze.179
  121.8 0.1 squeeze.180
  121.9 0.1 squeeze.182
  121.9 0.1 bitcast_maximum_fusion.3
  122.0 0.1 copy.100
  122.1 0.1 copy.99
  122.3 0.1 maximum_bitcast_fusion.2
  122.4 9.4 %all-gather.6 = f32[4,132,64]{1,2,0:T(8,128)S(1)} all-gather(f32[1,132,64]{1,2,0:T(8,128)S(1)} %maximum_bitcast_fusion.2), channel_id=4, replica_groups=mesh['gr'=2,'sp_0'=4,'sp_1'=4,'tp_0'=4,'tp_1'=2] {'tp_0'}, dimensions={0}, use_global_device_ids=true | all-gather | bytes 168960 | tf_op jit(solution)/shard_map/all_gather | solution.py:26
  131.7 0.1 fusion.82
  132.2 0.1 copy.110
  132.3 0.1 copy.109
  132.4 0.1 squeeze.200
  132.5 0.1 squeeze.195
  132.6 0.1 squeeze.196
  132.6 0.1 squeeze.198
  132.7 0.1 bitcast_maximum_fusion
  132.8 0.1 copy.114
  132.9 0.1 copy.113
  133.1 0.1 maximum_bitcast_fusion.3
  133.1 12.0 %all-gather.7 = f32[2,132,64]{1,2,0:T(8,128)S(1)} all-gather(f32[1,132,64]{1,2,0:T(8,128)S(1)} %maximum_bitcast_fusion.3), channel_id=5, replica_groups=mesh['gr'=2,'sp_0'=4,'sp_1'=4,'tp_0'=4,'tp_1'=2] {'tp_1'}, dimensions={0}, use_global_device_ids=true | all-gather | bytes 101376 | tf_op jit(solution)/shard_map/all_gather | solution.py:26
  145.2 0.1 fusion.85
  145.3 0.1 copy.125
  145.4 0.1 copy.124
  145.5 0.1 squeeze.215
  145.7 0.1 squeeze.214
  145.8 0.1 squeeze.211
  146.0 0.1 squeeze.212
  146.1 0.8 add_divide_fusion
  146.9 1.3 copy.130
  (50 shorter events, 1.8 us)
Async XLA Ops:
  0.6 95.5 %copy-start = (bf16[4,32,64]{2,1,0:T(8,128)(2,1)S(1)}, bf16[4,32,64]{2,1,0:T(8,128)(2,1)}, u32[]{:S(2)}) copy-start(bf16[4,32,64]{2,1,0:T(8,128)(2,1)} %param.10) | copy-start | bytes 49156
  0.6 5.3 %copy-start.2 = (bf16[2048,256]{1,0:T(8,128)(2,1)S(1)}, bf16[2048,256]{1,0:T(8,128)(2,1)}, u32[]{:S(2)}) copy-start(bf16[2048,256]{1,0:T(8,128)(2,1)} %param.9) | copy-start | bytes 3145732
  0.7 5.9 %copy-start.3 = (bf16[2048,256]{1,0:T(8,128)(2,1)S(1)}, bf16[2048,256]{1,0:T(8,128)(2,1)}, u32[]{:S(2)}) copy-start(bf16[2048,256]{1,0:T(8,128)(2,1)} %param.8) | copy-start | bytes 3145732
  5.9 1.4 copy-start.5
  15.8 7.1 %copy-start.1 = (bf16[4,512,2048]{2,1,0:T(8,128)(2,1)S(1)}, bf16[4,512,2048]{2,1,0:T(8,128)(2,1)}, u32[]{:S(2)}) copy-start(bf16[4,512,2048]{2,1,0:T(8,128)(2,1)} %fusion.2) | copy-start | bytes 25165828
  28.8 67.3 %copy-start.4 = (f32[1,1,8192]{2,1,0:T(1,128)S(1)}, f32[1,1,8192]{2,1,0:T(1,128)}, u32[]{:S(2)}) copy-start(f32[1,1,8192]{2,1,0:T(1,128)} %param.11) | copy-start | bytes 98308
  30.4 65.7 %all-to-all-start = ((bf16[128,1,64,128]{3,2,1,0:T(8,128)(2,1)}), bf16[128,1,64,128]{3,2,1,0:T(8,128)(2,1)S(1)}, u32[]{:S(2)}, u32[]{:S(2)}) async-start(bf16[128,1,64,128]{3,2,1,0:T(8,128)(2,1)} %bitcast.397), calls=%async_computation | async-start | bytes 4194304 | tf_op jit(solution)/shard_map/all_to_all | solution.py:76
where the time goes:
time: 148 us
  waiting for transfers between devices  51.9 us (35%)
  blocking collectives  41.8 us (28%)
  other arithmetic  16.7 us (11%)
  matrix products  13.8 us (9%)
  starting transfers between devices  13.8 us (9%)
  local copies, waits for them, and re-layouts  9.14 us (6%)
    all_to_all x1, waiting for transfers between devices, shards(): lax.all_to_all(stacked.reshape(sp_count * tp_count, 1, piece_len, 2 * HD)...  51.9 us
    all_gather x4, blocking collectives, collected_together(): both, at, found = (lax.all_gather(jnp.concatenate(lines), axis), 0, {})  41.8 us
    all_to_all x1, starting transfers between devices, shards(): lax.all_to_all(stacked.reshape(sp_count * tp_count, 1, piece_len, 2 * HD)...  13.8 us
    convert_element_type x1, other arithmetic, shards(): normed = (widened * inverse_rms * norm_gain).astype(jnp.bfloat16)  8.58 us
    dot_general x1, matrix products, shards(): jnp.einsum('gcbkd,dhe->gchbke', shaped, value_heads, preferred_element_ty...  7.06 us
    reduce_sum x1, other arithmetic, shards(): jnp.mean(widened * widened, axis=-1, keepdims=True) + NORM_FLOOR  5.23 us
    dot_general x1, matrix products, shards(): jnp.einsum('gcbkd,dhe->gchbke', shaped, key_heads, preferred_element_type...  4.72 us
  transfers between devices with their start and end apart: 1, of which 1 were waited for; matrix products, arithmetic and copies ran while one was open for 0% of the time, Pallas kernels for 0%

commit v1 on v0

--- a/solution.py
+++ b/solution.py
@@ -1,18 +1,146 @@
 import jax
 import jax.numpy as jnp
 from jax import lax
+from jax.experimental import pallas as pl
+from jax.experimental.pallas import tpu as pltpu
 from jax.sharding import Mesh
 from jax.sharding import PartitionSpec as P
 
 HD = 64
-SP = ("sp_0", "sp_1")
-TP = ("tp_0", "tp_1")
-SP_TP = ("sp_0", "sp_1", "tp_0", "tp_1")
+AXES = ("sp_0", "sp_1", "tp_0", "tp_1")
+SP_TP = AXES
+SP = AXES[:2]
+TP = AXES[2:]
 GR_SP = ("gr", "sp_0", "sp_1")
-
-
+MESH = pl.DeviceIdType.MESH
 NORM_FLOOR = 0.05
 SCORE_FLOOR = -1e30
+ROWS = 128
+STEPS = 16
+
+
+def across(z, kz):
+    flip = z + 1 - 2 * (z % 2)
+    return ((1 - kz % 2) * z + (kz % 2) * flip + 2 * (kz // 2)) % 4
+
+
+def peer_of(me, kz, kx, ky, kc):
+    z, x, y, c = me
+    return across(z, kz), (x + kx) % 4, (y + ky) % 4, (c + kc) % 2
+
+
+def device_of(t):
+    return dict(zip(AXES, t))
+
+
+def slot_of(t):
+    return t[0] * 32 + t[1] * 8 + t[2] * 2 + t[3]
+
+
+def cache_kernel(
+    tok_hbm, gain_ref, wk_hbm, wv_hbm, kv_hbm,
+    tok, wk, wv, normed, made, tok_sem, w_sem, self_sem, send_sem, recv_sem,
+):
+    me = tuple(lax.axis_index(a) for a in AXES)
+    mine = slot_of(me)
+    wk_copy = pltpu.make_async_copy(wk_hbm, wk, w_sem.at[0])
+    wv_copy = pltpu.make_async_copy(wv_hbm, wv, w_sem.at[1])
+
+    def rel(i):
+        return 3 - i % 4, (i // 4 + 1) % 4
+
+    def tok_copy(i):
+        kz, kx = rel(i)
+        rows = pl.ds(pl.multiple_of((me[1] + kx) % 4 * ROWS, ROWS), ROWS)
+        return pltpu.make_async_copy(
+            tok_hbm.at[across(me[0], kz), rows], tok.at[i], tok_sem.at[i]
+        )
+
+    tok_copy(0).start()
+    wk_copy.start()
+    wv_copy.start()
+
+    @pl.loop(1, STEPS)
+    def _(i):
+        tok_copy(i).start()
+
+    barrier = pltpu.get_barrier_semaphore()
+
+    @pl.loop(1, 128)
+    def _(n):
+        k = 128 - n
+        to = peer_of(me, k // 32, k // 8 % 4, k // 2 % 4, k % 2)
+        pl.semaphore_signal(barrier, inc=1, device_id=device_of(to), device_id_type=MESH)
+
+    wk_copy.wait()
+    wv_copy.wait()
+
+    @pl.loop(0, STEPS)
+    def _(i):
+        kz, kx = rel(i)
+        tok_copy(i).wait()
+
+        for r in range(0, ROWS, 16):
+            wide = tok[i, pl.ds(r, 16)].astype(jnp.float32)
+            mean = jnp.sum(wide * wide, axis=-1, keepdims=True) * (1.0 / wide.shape[-1])
+            scale = lax.rsqrt(mean + NORM_FLOOR)
+            normed[pl.ds(r, 16)] = (wide * scale * gain_ref[...]).astype(jnp.bfloat16)
+
+        keys = jnp.dot(normed[...], wk[...], preferred_element_type=jnp.float32)
+        values = jnp.dot(normed[...], wv[...], preferred_element_type=jnp.float32)
+        base = across(me[0], kz) * 32 + (me[1] + kx) % 4 * 8
+        for h in range(4):
+            cols = slice(h * HD, (h + 1) * HD)
+            both = jnp.concatenate([keys[:, cols], values[:, cols]], axis=1).astype(jnp.bfloat16)
+            made[base + 2 * h] = both[:64]
+            made[base + 2 * h + 1] = both[64:]
+
+        @pl.when(i == 0)
+        def _():
+            pl.semaphore_wait(barrier, 127)
+
+        @pl.loop(0, 8)
+        def _(j):
+            to = peer_of(me, kz, kx, j // 2, j % 2)
+
+            @pl.when(i * 8 + j != 120)
+            def _():
+                pltpu.make_async_remote_copy(
+                    made.at[slot_of(to)], kv_hbm.at[mine], send_sem, recv_sem,
+                    device_id=device_of(to), device_id_type=MESH,
+                ).start()
+
+    own = pltpu.make_async_copy(made.at[mine], kv_hbm.at[mine], self_sem)
+    own.start()
+    own.wait()
+    some = pl.ds(0, 127)
+    pltpu.make_async_copy(made.at[some], kv_hbm.at[some], recv_sem).wait()
+    pltpu.make_async_copy(made.at[some], kv_hbm.at[some], send_sem).wait()
+
+
+def make_cache(tokens, norm_gain, w_key, w_value):
+    width = tokens.shape[-1]
+    any_space = pl.BlockSpec(memory_space=pl.ANY)
+    return pl.pallas_call(
+        cache_kernel,
+        out_shape=jax.ShapeDtypeStruct((128, 64, 2 * HD), jnp.bfloat16),
+        in_specs=[any_space, pl.BlockSpec(memory_space=pltpu.VMEM), any_space, any_space],
+        out_specs=any_space,
+        scratch_shapes=[
+            pltpu.VMEM((STEPS, ROWS, width), jnp.bfloat16),
+            pltpu.VMEM(w_key.shape, jnp.bfloat16),
+            pltpu.VMEM(w_value.shape, jnp.bfloat16),
+            pltpu.VMEM((ROWS, width), jnp.bfloat16),
+            pltpu.VMEM((128, 64, 2 * HD), jnp.bfloat16),
+            pltpu.SemaphoreType.DMA((STEPS,)),
+            pltpu.SemaphoreType.DMA((2,)),
+            pltpu.SemaphoreType.DMA,
+            pltpu.SemaphoreType.DMA,
+            pltpu.SemaphoreType.DMA,
+        ],
+        compiler_params=pltpu.CompilerParams(collective_id=0, has_side_effects=True),
+        cost_estimate=pl.CostEstimate(flops=4_300_000_000, bytes_accessed=14_000_000, transcendentals=0),
+    )(tokens, norm_gain.reshape(1, -1), w_key, w_value)
 
 
 def collected_together(array, axis):
@@ -60,26 +188,7 @@
     classes = sp_count // seq_count
     halves = tp_count // kv_heads
     piece_len = positions // (classes * halves)
-    widened = tokens.astype(jnp.float32)
-    inverse_rms = lax.rsqrt(jnp.mean(widened * widened, axis=-1, keepdims=True) + NORM_FLOOR)
-    normed = (widened * inverse_rms * norm_gain).astype(jnp.bfloat16)
-    shaped = normed.reshape(seq_count, classes, halves, piece_len, model_width)
-    key_heads = w_key.reshape(model_width, kv_heads, HD)
-    value_heads = w_value.reshape(model_width, kv_heads, HD)
-    keys_made = jnp.einsum(
-        "gcbkd,dhe->gchbke", shaped, key_heads, preferred_element_type=jnp.float32
-    ).astype(jnp.bfloat16)
-    values_made = jnp.einsum(
-        "gcbkd,dhe->gchbke", shaped, value_heads, preferred_element_type=jnp.float32
-    ).astype(jnp.bfloat16)
-    stacked = jnp.concatenate([keys_made, values_made], axis=-1)
-    arrived = lax.all_to_all(
-        stacked.reshape(sp_count * tp_count, 1, piece_len, 2 * HD),
-        SP_TP,
-        split_axis=0,
-        concat_axis=1,
-        tiled=True,
-    )
+    arrived = make_cache(tokens, norm_gain, w_key, w_value)
     kv_cache = arrived.reshape(1, 1, sp_count * tp_count * piece_len, 2 * HD)
     query_heads = new_query.shape[1]
     group_size = query_heads // kv_heads

time: 148 us -> 120 us (0.81)
  Pallas kernels: 0 us -> 65.9 us
  waiting for transfers between devices: 51.9 us -> 0 us
  other arithmetic: 16.7 us -> 1.69 us
  starting transfers between devices: 13.8 us -> 0 us
  matrix products: 13.8 us -> 3.81 us
  local copies, waits for them, and re-layouts: 9.14 us -> 6.34 us
    pallas_call x0 -> x1, Pallas kernels: none -> 65.9 us  [make_cache(): pl.pallas_call(cache_kernel, out_shape=jax.ShapeDtypeStruct((128, 64, 2 *...]
    all_to_all x1 -> x0, waiting for transfers between devices: 51.9 us -> none  [shards(): lax.all_to_all(stacked.reshape(sp_count * tp_count, 1, piece_len, 2 * HD)...]
    all_to_all x1 -> x0, starting transfers between devices: 13.8 us -> none  [shards(): lax.all_to_all(stacked.reshape(sp_count * tp_count, 1, piece_len, 2 * HD)...]
    dot_general x2 -> x0, matrix products: 11.8 us -> none  [the longest x1 7.06 us: shards(): jnp.einsum('gcbkd,dhe->gchbke', shaped, value_heads, preferred_element_ty...]
    convert_element_type x1 -> x0, other arithmetic: 8.58 us -> none  [shards(): normed = (widened * inverse_rms * norm_gain).astype(jnp.bfloat16)]
    reduce_sum x1 -> x0, other arithmetic: 5.23 us -> none  [shards(): jnp.mean(widened * widened, axis=-1, keepdims=True) + NORM_FLOOR]
    dot_general x1, matrix products: 0.76 us -> 2.5 us  [shards(): lax.dot_general(queries, keys_here, (((1,), (1,)), ((), ())), preferred_e...]
    concatenate x1 -> x0, local copies, waits for them, and re-layouts: 1.58 us -> none  [shards(): stacked = jnp.concatenate([keys_made, values_made], axis=-1)]
  transfers between devices with their start and end apart: 1 -> 0, of which waited for: 1 -> 0; matrix products, arithmetic and copies ran while one was open for 0% -> 0% of each run, Pallas kernels for 0% -> 0%
where the time goes in v1:
time: 120 us; the launch traced here: 119 us
  Pallas kernels  65.9 us (55%)
  blocking collectives  40.7 us (34%)
  local copies, waits for them, and re-layouts  6.34 us (5%)
  matrix products  3.81 us (3%)
  other arithmetic  1.69 us (1%)
    pallas_call x1, Pallas kernels, make_cache(): pl.pallas_call(cache_kernel, out_shape=jax.ShapeDtypeStruct((128, 64, 2 *...  65.9 us
    all_gather x4, blocking collectives, collected_together(): both, at, found = (lax.all_gather(jnp.concatenate(lines), axis), 0, {})  40.7 us
    dot_general x1, matrix products, shards(): lax.dot_general(queries, keys_here, (((1,), (1,)), ((), ())), preferred_e...  2.5 us

profile of v1, /device:TPU:1, one launch (start us, length us, event | category | flops | bytes accessed | tf_op | source)
XLA Modules:
  0.0 119.4 jit_solution(4336862665818484510)
XLA Ops:
  0.7 65.9 %shard_map.77 = bf16[128,64,128]{2,1,0:T(8,128)(2,1)} custom-call(bf16[4,512,2048]{2,1,0:T(8,128)(2,1)} %tok_hbm.1, f32[1,2048]{1,0:T(1,128)} %bitcast.376, bf16[2048,256]{1,0:T(8,128)(2,1)} %wk_hbm.1, bf16[2048,256]{1,0:T(8,128)(2,1)} %wv_hbm.1), custom_call_target="tpu_custom_call" | custom-call | flops 4300000256 | bytes 14000000 | tf_op jit(solution)/shard_map/pallas_call | solution.py:124
  66.6 2.5 %fusion.84 = (f32[8]{0:T(128)S(1)}, f32[8,8192]{1,0:T(8,128)S(1)}) fusion(f32[8192]{0:T(1024)S(1)} %bitcast.373, bf16[1,1,8192,128]{3,2,1,0:T(8,128)(2,1)} %bitcast.367, bf16[4,32,64]{2,1,0:T(8,128)(2,1)S(1)} %copy-done, s32[]{:T(128)S(6)} %select_n.21, s32[]{:T(128)S(6)} %select_n.23), kind=kOutput, calls=%fused_computation.157 | convolution fusion | flops 8585208 | bytes 2394152 | tf_op jit(solution)/shard_map/dot_general | solution.py:202
  69.2 1.3 %fusion.3 = f32[4,32,64]{2,1,0:T(8,128)S(1)} fusion(f32[4,32,64]{2,1,0:T(8,128)S(1)} %broadcast_in_dim.12, s32[]{:T(128)S(6)} %select_n.21, s32[]{:T(128)S(6)} %select_n.23, bf16[1,1,8192,128]{3,2,1,0:T(8,128)(2,1)S(1)} %bitcast.368, f32[8,8192]{1,0:T(8,128)S(1)} %get-tuple-element.63, f32[8]{0:T(128)S(1)} %get-tuple-element.62), kind=kOutput, calls=%fused_computation.6 | convolution fusion | flops 50397184 | bytes 2363912 | tf_op jit(solution)/shard_map/dot_general | solution.py:209
  70.5 0.3 fusion.4
  70.8 0.2 dynamic_update_slice.11
  70.9 0.1 reshape.527
  71.0 0.1 dynamic_update_slice.10
  71.1 0.1 reshape.526
  71.2 0.1 copy.59
  71.3 10.9 %all-gather.4 = f32[4,132,64]{1,2,0:T(8,128)S(1)} all-gather(f32[1,132,64]{1,2,0:T(8,128)S(1)} %copy.59), channel_id=2, replica_groups=mesh['gr'=2,'sp_0'=4,'sp_1'=4,'tp_0'=4,'tp_1'=2] {'sp_0'}, dimensions={0}, use_global_device_ids=true | all-gather | bytes 168960 | tf_op jit(solution)/shard_map/all_gather | solution.py:154
  82.2 0.1 fusion.81
  82.3 0.1 copy.60
  82.4 0.1 squeeze.163
  82.5 0.1 copy.61
  82.6 0.1 squeeze.164
  82.6 0.1 copy.62
  82.7 0.1 squeeze.166
  82.8 0.1 copy.63
  82.9 0.1 squeeze.168
  83.1 0.1 copy.68
  83.1 0.1 copy.69
  83.2 0.1 copy.70
  83.3 0.1 copy.71
  83.4 0.1 copy.72
  83.5 0.1 copy.73
  83.6 0.1 maximum_bitcast_fusion.1
  83.7 9.4 %all-gather.5 = f32[4,132,64]{1,2,0:T(8,128)S(1)} all-gather(f32[1,132,64]{1,2,0:T(8,128)S(1)} %maximum_bitcast_fusion.1), channel_id=3, replica_groups=mesh['gr'=2,'sp_0'=4,'sp_1'=4,'tp_0'=4,'tp_1'=2] {'sp_1'}, dimensions={0}, use_global_device_ids=true | all-gather | bytes 168960 | tf_op jit(solution)/shard_map/all_gather | solution.py:154
  93.0 0.1 fusion.80
  93.1 0.1 copy.74
  93.2 0.1 squeeze.179
  93.3 0.1 copy.75
  93.4 0.1 squeeze.180
  93.4 0.1 copy.76
  93.5 0.1 squeeze.182
  93.6 0.1 copy.77
  93.7 0.1 squeeze.184
  93.9 0.1 copy.82
  93.9 0.1 copy.83
  94.2 0.1 copy.86
  94.3 0.1 copy.87
  94.4 0.1 maximum_bitcast_fusion.2
  94.5 9.7 %all-gather.6 = f32[4,132,64]{1,2,0:T(8,128)S(1)} all-gather(f32[1,132,64]{1,2,0:T(8,128)S(1)} %maximum_bitcast_fusion.2), channel_id=4, replica_groups=mesh['gr'=2,'sp_0'=4,'sp_1'=4,'tp_0'=4,'tp_1'=2] {'tp_0'}, dimensions={0}, use_global_device_ids=true | all-gather | bytes 168960 | tf_op jit(solution)/shard_map/all_gather | solution.py:154
  104.1 0.1 fusion.79
  104.2 0.1 copy.88
  104.3 0.1 squeeze.195
  104.5 0.1 squeeze.196
  104.5 0.1 copy.90
  104.6 0.1 squeeze.198
  104.8 0.1 squeeze.200
  105.0 0.1 copy.96
  105.3 0.1 copy.100
  105.4 0.1 copy.101
  105.5 0.1 maximum_bitcast_fusion.3
  105.6 10.8 %all-gather.7 = f32[2,132,64]{1,2,0:T(8,128)S(1)} all-gather(f32[1,132,64]{1,2,0:T(8,128)S(1)} %maximum_bitcast_fusion.3), channel_id=5, replica_groups=mesh['gr'=2,'sp_0'=4,'sp_1'=4,'tp_0'=4,'tp_1'=2] {'tp_1'}, dimensions={0}, use_global_device_ids=true | all-gather | bytes 101376 | tf_op jit(solution)/shard_map/all_gather | solution.py:154
  116.4 0.1 fusion.82
  116.4 0.1 copy.103
  116.5 0.1 squeeze.211
  116.7 0.1 squeeze.212
  116.8 0.1 squeeze.214
  117.0 0.1 squeeze.215
  117.1 0.1 copy.108
  117.2 0.1 copy.109
  117.3 0.8 add_divide_fusion
  118.1 1.3 %copy.114 = bf16[1,1,8192,128]{3,2,1,0:T(8,128)(2,1)} copy(bf16[1,1,8192,128]{3,2,1,0:T(8,128)(2,1)S(1)} %bitcast.369) | data formatting | bytes 4194304
  (34 shorter events, 1.2 us)
Async XLA Ops:
  0.6 66.0 %copy-start = (bf16[4,32,64]{2,1,0:T(8,128)(2,1)S(1)}, bf16[4,32,64]{2,1,0:T(8,128)(2,1)}, u32[]{:S(2)}) copy-start(bf16[4,32,64]{2,1,0:T(8,128)(2,1)} %param.10) | copy-start | bytes 49156
  0.7 66.0 %copy-start.2 = (f32[1,1,8192]{2,1,0:T(1,128)S(1)}, f32[1,1,8192]{2,1,0:T(1,128)}, u32[]{:S(2)}) copy-start(f32[1,1,8192]{2,1,0:T(1,128)} %param.11) | copy-start | bytes 98308
  66.6 2.6 %copy-start.1 = (bf16[128,64,128]{2,1,0:T(8,128)(2,1)S(1)}, bf16[128,64,128]{2,1,0:T(8,128)(2,1)}, u32[]{:S(2)}) copy-start(bf16[128,64,128]{2,1,0:T(8,128)(2,1)} %shard_map.77) | copy-start | bytes 6291460

commit v2 on v1

v2 whole, which is shorter than its diff:
```python
import jax
import jax.numpy as jnp
from jax import lax
from jax.experimental import pallas as pl
from jax.experimental.pallas import tpu as pltpu
from jax.sharding import Mesh
from jax.sharding import PartitionSpec as P

HD = 64
AXES = ("z", "x", "y", "core")
SP, TP = AXES[:2], AXES[2:]
MESH = pl.DeviceIdType.MESH
NORM_FLOOR = 0.05
ROWS = 128
STEPS = 16
BURST = 5
DEPTH = 4
KV = (((1,), (1,)), ((), ()))


def across(z, kz):
    flip = z + 1 - 2 * (z % 2)
    return ((1 - kz % 2) * z + (kz % 2) * flip + 2 * (kz // 2)) % 4


def peer_of(me, kz, kx, ky, kc):
    z, x, y, c = me
    return across(z, kz), (x + kx) % 4, (y + ky) % 4, (c + kc) % 2


def step_of(i):
    j = i % 4
    return 3 - (j % 2 * 2 + j // 2), (i // 4 + j + 2) % 4


def device_of(t):
    return dict(zip(AXES, t))


def send(src, dst, send_sem, recv_sem, to):
    pltpu.make_async_remote_copy(
        src, dst, send_sem, recv_sem, device_id=device_of(to), device_id_type=MESH
    ).start()


def await_bytes(like, sem):
    pltpu.make_async_copy(like, like, sem).wait()


def merged(parts, lane):
    tops = [p[:, :1] for p in parts]
    top = tops[0]
    for t in tops[1:]:
        top = jnp.maximum(top, t)
    total = sum(jnp.exp(t - top) * p for t, p in zip(tops, parts))
    return jnp.where(lane == 0, top, total)


def kernel(
    tok_hbm, gain_hbm, wk_hbm, wv_hbm, query_hbm, gate_hbm, kv_hbm, read_hbm,
    tok, gain, wk, wv, query, padded, normed, made, gates, packed,
    part, part_in, row, row_in, final, final_in, read_in, lined, read,
    tok_sem, in_sem, wave_sem, send_sem, recv_sem,
):
    me = tuple(lax.axis_index(a) for a in AXES)
    z, x, y, core = me
    chip = z * 16 + x * 4 + y
    mine = chip * 2 + core
    sp, tp = z * 4 + x, y * 2 + core

    def tok_copy(i):
        kz, kx = step_of(i)
        rows = pl.ds(pl.multiple_of((x + kx) % 4 * ROWS, ROWS), ROWS)
        return pltpu.make_async_copy(tok_hbm.at[across(z, kz), rows], tok.at[i], tok_sem.at[i])

    in_copies = [
        pltpu.make_async_copy(src, dst, in_sem.at[n])
        for n, (src, dst) in enumerate((
            (wk_hbm, wk), (wv_hbm, wv), (gain_hbm, gain), (query_hbm, query),
            (gate_hbm.at[chip], gates.at[core * 64 + chip]),
        ))
    ]
    tok_copy(0).start()
    for copy in in_copies:
        copy.start()

    @pl.loop(1, STEPS)
    def _(i):
        tok_copy(i).start()

    barrier = pltpu.get_barrier_semaphore()

    @pl.loop(1, 128)
    def _(n):
        k = 128 - n
        to = peer_of(me, k // 32, k // 8 % 4, k // 2 % 4, k % 2)
        pl.semaphore_signal(barrier, inc=1, device_id=device_of(to), device_id_type=MESH)

    def send_step(i):
        kz, kx = step_of(i)

        @pl.loop(0, 8)
        def _(j):
            to = peer_of(me, kz, kx, j // 2, j % 2)

            @pl.when(i * 8 + j != (STEPS - 1) * 8)
            def _():
                slot = to[0] * 32 + to[1] * 8 + to[2] * 2 + to[3]
                send(made.at[slot], kv_hbm.at[mine], wave_sem.at[i], recv_sem.at[0], to)

    def await_step(i, n=8):
        await_bytes(made.at[pl.ds(0, n)], wave_sem.at[i])

    def send_gates():
        @pl.loop(1, 64)
        def _(k):
            to = peer_of(me, k // 16, k // 4 % 4, k % 4, 0)
            send(
                gate_hbm.at[to[0] * 16 + to[1] * 4 + to[2]], gates.at[core * 64 + chip],
                send_sem.at[0], recv_sem.at[1], to,
            )

    mate = (z, x, y, 1 - core)

    for copy in in_copies:
        copy.wait()

    @pl.loop(0, STEPS)
    def _(i):
        kz, kx = step_of(i)
        tok_copy(i).wait()
        for r in range(0, ROWS, 16):
            wide = tok[i, pl.ds(r, 16)].astype(jnp.float32)
            mean = jnp.sum(wide * wide, axis=-1, keepdims=True) * (1.0 / wide.shape[-1])
            scale = lax.rsqrt(mean + NORM_FLOOR)
            normed[pl.ds(r, 16)] = (wide * scale * gain[...]).astype(jnp.bfloat16)

        keys = jnp.dot(normed[...], wk[...], preferred_element_type=jnp.float32)
        values = jnp.dot(normed[...], wv[...], preferred_element_type=jnp.float32)
        base = across(z, kz) * 32 + (x + kx) % 4 * 8
        for h in range(4):
            cols = slice(h * HD, (h + 1) * HD)
            both = jnp.concatenate([keys[:, cols], values[:, cols]], axis=1).astype(jnp.bfloat16)
            made[base + 2 * h] = both[:64]
            made[base + 2 * h + 1] = both[64:]

        @pl.when(i == 0)
        def _():
            pl.semaphore_wait(barrier, 127)

        @pl.when(i < BURST)
        def _():
            send_step(i)

        @pl.when(i == 0)
        def _():
            send_gates()

        @pl.when(i == 8)
        def _():
            await_bytes(gates.at[pl.ds(0, 63)], recv_sem.at[1])
            held = gates.at[pl.ds(core * 64, 64)]
            send(held, held, send_sem.at[1], recv_sem.at[2], mate)

    own = pltpu.make_async_copy(made.at[mine], kv_hbm.at[mine], in_sem.at[0])
    own.start()

    lane = lax.broadcasted_iota(jnp.int32, (8, 2 * HD), 1)
    lane16 = lax.broadcasted_iota(jnp.int32, (16, 2 * HD), 1)
    for g in range(4):
        wide = query[g].astype(jnp.float32)
        both = jnp.concatenate([wide, jnp.zeros_like(wide)], axis=1)
        for h in range(4):
            padded[g * 4 + h] = both[h * 8 : (h + 1) * 8]

    await_bytes(gates.at[pl.ds(0, 64)], recv_sem.at[2])

    @pl.loop(0, 4)
    def _(g):
        for h in range(4):
            for c in range(4):
                for b in range(2):
                    packed[b, h * 4 + c : h * 4 + c + 1] = gates[b * 64 + g * 16 + c * 4 + h]
        low, high = packed[0], packed[1]
        low_turned, high_turned = (
            jnp.concatenate([t[:, HD:], t[:, :HD]], axis=1) for t in (low, high)
        )
        gate = jnp.where(
            lane16 < HD,
            jnp.where(core == 0, low, low_turned),
            jnp.where(core == 0, high_turned, high),
        )
        for h in range(4):
            q = padded[g * 4 + h].astype(jnp.bfloat16)
            pieces = [
                made[pl.ds(g * 32 + c * 8 + h * 2, 2)].reshape(ROWS, 2 * HD) for c in range(4)
            ]
            score = jnp.concatenate(
                [
                    lax.dot_general(q, p, KV, preferred_element_type=jnp.float32) * HD ** (-0.5)
                    - gate[h * 4 + c : h * 4 + c + 1]
                    for c, p in enumerate(pieces)
                ],
                axis=1,
            )
            top = jnp.max(score, axis=1, keepdims=True)
            weight = jnp.exp(score - top)
            total = jnp.sum(weight, axis=1, keepdims=True)
            first = weight.astype(jnp.bfloat16).astype(jnp.float32)
            second = (weight - first).astype(jnp.bfloat16).astype(jnp.float32)
            third = weight - first - second
            split = jnp.concatenate([first, second, third], axis=0).astype(jnp.bfloat16)
            out = jnp.dot(
                split, jnp.concatenate(pieces, axis=0), preferred_element_type=jnp.float32
            )
            out = out[:8] + out[8:16] + out[16:]
            part[g * 4 + h] = jnp.where(lane == 0, top, jnp.where(lane < HD, total, out))

    def send_part():
        @pl.loop(1, 8)
        def _(k):
            to = peer_of(me, 0, 0, k // 2, k % 2)
            send(
                part.at[pl.ds((to[2] * 2 + to[3]) * 2, 2)], part_in.at[pl.ds(tp * 2, 2)],
                send_sem.at[2], recv_sem.at[3], to,
            )

    def send_row():
        await_bytes(part_in.at[pl.ds(0, 14)], recv_sem.at[3])
        for n in range(2):
            part_in[tp * 2 + n] = part[tp * 2 + n]
        for n in range(2):
            one = merged([part_in[t * 2 + n] for t in range(8)], lane)
            for j in range(8):
                row[n * 8 + j] = one[j : j + 1]

        @pl.loop(1, 16)
        def _(k):
            to = peer_of(me, k // 4, k % 4, 0, 0)
            send(row.at[to[0] * 4 + to[1]], row_in.at[sp], send_sem.at[3], recv_sem.at[4], to)

    def send_final():
        await_bytes(row_in.at[pl.ds(0, 15)], recv_sem.at[4])
        row_in[sp] = row[sp]
        one = merged([row_in[s] for s in range(16)], lane[:1])
        done = one / one[:, 1:2]
        final[0] = done
        final_in[sp] = done

        @pl.loop(1, 16)
        def _(k):
            to = peer_of(me, k // 4, k % 4, 0, 0)
            send(final.at[0], final_in.at[sp], send_sem.at[4], recv_sem.at[5], to)

    def send_read():
        await_bytes(final_in.at[pl.ds(0, 15)], recv_sem.at[5])
        for s in range(16):
            read_in[tp, s] = final_in[s]

        @pl.loop(1, 8)
        def _(k):
            to = peer_of(me, 0, 0, k // 2, k % 2)
            send(final_in, read_in.at[tp], send_sem.at[5], recv_sem.at[6], to)

    send_part()

    @pl.loop(BURST, STEPS)
    def _(i):
        await_step(i - DEPTH)
        send_step(i)
        pl.when(i == 7)(send_row)
        pl.when(i == 9)(send_final)
        pl.when(i == 11)(send_read)

    await_bytes(read_in.at[pl.ds(0, 7)], recv_sem.at[6])
    for t in range(8):
        for s in range(16):
            lined[s : s + 1] = read_in[t, s]
        read[t // 2, t % 2 * 16 : t % 2 * 16 + 16] = lined[...][:, HD:]
    out_copy = pltpu.make_async_copy(read, read_hbm, in_sem.at[1])
    out_copy.start()

    await_step(0)
    for i in range(STEPS - DEPTH, STEPS):
        await_step(i, 7 if i == STEPS - 1 else 8)
    await_bytes(gates.at[pl.ds(0, 63)], send_sem.at[0])
    await_bytes(gates.at[pl.ds(0, 64)], send_sem.at[1])
    await_bytes(part_in.at[pl.ds(0, 14)], send_sem.at[2])
    await_bytes(row_in.at[pl.ds(0, 15)], send_sem.at[3])
    await_bytes(final_in.at[pl.ds(0, 15)], send_sem.at[4])
    await_bytes(read_in.at[pl.ds(0, 7)], send_sem.at[5])
    own.wait()
    out_copy.wait()
    pltpu.make_async_copy(made.at[pl.ds(0, 127)], kv_hbm.at[pl.ds(0, 127)], recv_sem.at[0]).wait()


def shards(tokens, norm_gain, w_key, w_value, new_query, cum_gate):
    width = tokens.shape[-1]
    lanes = 2 * HD
    bf16, f32 = jnp.bfloat16, jnp.float32
    kv_cache, first_read = pl.pallas_call(
        kernel,
        out_shape=[
            jax.ShapeDtypeStruct((128, 64, lanes), bf16),
            jax.ShapeDtypeStruct(new_query.shape, f32),
        ],
        in_specs=[pl.BlockSpec(memory_space=pl.ANY)] * 6,
        out_specs=[pl.BlockSpec(memory_space=pl.ANY)] * 2,
        scratch_shapes=[
            pltpu.VMEM((STEPS, ROWS, width), bf16),
            pltpu.VMEM((1, width), f32),
            pltpu.VMEM(w_key.shape, bf16),
            pltpu.VMEM(w_value.shape, bf16),
            pltpu.VMEM(new_query.shape, bf16),
            pltpu.VMEM((16, 8, lanes), f32),
            pltpu.VMEM((ROWS, width), bf16),
            pltpu.VMEM((128, 64, lanes), bf16),
            pltpu.VMEM((128, 1, lanes), f32),
            pltpu.VMEM((2, 16, lanes), f32),
            pltpu.VMEM((16, 8, lanes), f32),
            pltpu.VMEM((16, 8, lanes), f32),
            pltpu.VMEM((16, 1, lanes), f32),
            pltpu.VMEM((16, 1, lanes), f32),
            pltpu.VMEM((1, 1, lanes), f32),
            pltpu.VMEM((16, 1, lanes), f32),
            pltpu.VMEM((8, 16, 1, lanes), f32),
            pltpu.VMEM((16, lanes), f32),
            pltpu.VMEM(new_query.shape, f32),
            pltpu.SemaphoreType.DMA((STEPS,)),
            pltpu.SemaphoreType.DMA((5,)),
            pltpu.SemaphoreType.DMA((STEPS,)),
            pltpu.SemaphoreType.DMA((6,)),
            pltpu.SemaphoreType.DMA((7,)),
        ],
        compiler_params=pltpu.CompilerParams(collective_id=0, has_side_effects=True),
    )(
        tokens, norm_gain.reshape(1, width), w_key, w_value, new_query,
        cum_gate.reshape(64, 1, lanes),
    )
    return kv_cache.reshape(1, 1, 128 * 64, lanes), first_read


def solution(mesh):
    split = Mesh(mesh.devices.reshape(mesh.shape["gr"], 4, 4, 4, 2), ("gr", *AXES))
    return jax.shard_map(
        shards,
        mesh=split,
        in_specs=(
            P("gr", (*SP, *TP), None), P(), P(), P(), P("gr", None, None), P(("gr", *SP), TP, None)
        ),
        out_specs=(P(("gr", *SP), TP, None, None), P("gr", None, None)),
        check_vma=False,
    )
```

time: 120 us -> 72.9 us (0.61)
  blocking collectives: 40.7 us -> 0 us
  matrix products: 3.81 us -> 0 us
  local copies, waits for them, and re-layouts: 6.34 us -> 3.71 us
  Pallas kernels: 65.9 us -> 68.2 us
  other arithmetic: 1.69 us -> 0 us
    all_gather x4 -> x0, blocking collectives: 40.7 us -> none  [collected_together(): both, at, found = (lax.all_gather(jnp.concatenate(lines), axis), 0, {})]
    dot_general x2 -> x0, matrix products: 3.81 us -> none  [the longest x1 2.5 us: shards(): lax.dot_general(queries, keys_here, (((1,), (1,)), ((), ())), preferred_e...]
    slice x33 -> x0, local copies, waits for them, and re-layouts: 2.38 us -> none  [the longest x21 1.54 us: merged_by_axis(): array = combine(array, jax.tree.map(lambda part: part[k], pieces))]
    pallas_call x1, Pallas kernels: 65.9 us -> 68.2 us  [shards(): pl.pallas_call(kernel, out_shape=[jax.ShapeDtypeStruct((128, 64, lanes),...]
    unnamed x10 -> x4, local copies, waits for them, and re-layouts: 1.6 us -> 3.71 us
    squeeze x16 -> x0, local copies, waits for them, and re-layouts: 1.35 us -> none  [the longest x11 0.93 us: merged_by_axis(): array = combine(array, jax.tree.map(lambda part: part[k], pieces))]
where the time goes in v2:
time: 72.9 us; the launch traced here: 72.5 us
  Pallas kernels  68.2 us (94%)
  local copies, waits for them, and re-layouts  3.71 us (5%)
    pallas_call x1, Pallas kernels, shards(): pl.pallas_call(kernel, out_shape=[jax.ShapeDtypeStruct((128, 64, lanes),...  68.2 us
    unnamed x4, local copies, waits for them, and re-layouts  3.71 us

profile of v2, /device:TPU:1, one launch (start us, length us, event | category | flops | bytes accessed | tf_op | source)
XLA Modules:
  0.0 72.5 jit_solution(774443260442480258)
XLA Ops:
  0.6 68.2 %shard_map.77 = (bf16[128,64,128]{2,1,0:T(8,128)(2,1)}, f32[4,32,64]{2,1,0:T(8,128)}) custom-call(bf16[4,512,2048]{2,1,0:T(8,128)(2,1)} %tok_hbm.1, f32[1,2048]{1,0:T(1,128)} %bitcast.5, bf16[2048,256]{1,0:T(8,128)(2,1)} %wk_hbm.1, bf16[2048,256]{1,0:T(8,128)(2,1)} %wv_hbm.1, bf16[4,32,64]{2,1,0:T(8,128)(2,1)} %query_hbm.1, f32[64,1,128]{2,1,0:T(1,128)} %bitcast.4), custom_call_target="tpu_custom_call" | custom-call | tf_op jit(solution)/shard_map/pallas_call | solution.py:301
  68.8 0.0 copy-start
  68.8 3.1 %copy.10 = bf16[1,1,8192,128]{3,2,1,0:T(8,128)(2,1)} copy(bf16[1,1,8192,128]{3,2,1,0:T(8,128)(2,1)} %bitcast.3) | data formatting | bytes 4194304
  71.9 0.0 copy-done
  71.9 0.6 copy.11
Async XLA Ops:
  68.8 3.1 %copy-start = (f32[4,32,64]{2,1,0:T(8,128)S(1)}, f32[4,32,64]{2,1,0:T(8,128)}, u32[]{:S(2)}) copy-start(f32[4,32,64]{2,1,0:T(8,128)} %get-tuple-element.9) | copy-start | bytes 98308

commit v3 on v2

v3 whole, which is shorter than its diff:
```python
import jax
import jax.numpy as jnp
from jax import lax
from jax.experimental import pallas as pl
from jax.experimental.pallas import tpu as pltpu
from jax.sharding import Mesh
from jax.sharding import PartitionSpec as P

HD = 64
AXES = ("z", "x", "y", "core")
SP, TP = AXES[:2], AXES[2:]
MESH = pl.DeviceIdType.MESH
NORM_FLOOR = 0.05
ROWS = 128
STEPS = 16
BURST = 8
DEPTH = 4
KV = (((1,), (1,)), ((), ()))


def across(z, kz):
    flip = z + 1 - 2 * (z % 2)
    return ((1 - kz % 2) * z + (kz % 2) * flip + 2 * (kz // 2)) % 4


def step_of(i):
    j = i % 4
    return 3 - (j % 2 * 2 + j // 2), (i // 4 + j + 2) % 4


def device_of(t):
    return dict(zip(AXES, t))


def send(src, dst, send_sem, recv_sem, to):
    pltpu.make_async_remote_copy(
        src, dst, send_sem, recv_sem, device_id=device_of(to), device_id_type=MESH
    ).start()


def await_bytes(like, sem):
    pltpu.make_async_copy(like, like, sem).wait()


def merged(parts, lane):
    tops = [p[:, :1] for p in parts]
    top = tops[0]
    for t in tops[1:]:
        top = jnp.maximum(top, t)
    total = sum(jnp.exp(t - top) * p for t, p in zip(tops, parts))
    return jnp.where(lane == 0, top, total)


def kernel(
    tok_hbm, gain_hbm, wk_hbm, wv_hbm, query_hbm, gate_hbm, cache, read,
    tok, gain, wk, wv, query, padded, normed, made, gates, packed,
    part, part_in, row, row_in, final, final_in, read_in, lined,
    tok_sem, in_sem, wave_sem, send_sem, recv_sem,
):
    me = tuple(lax.axis_index(a) for a in AXES)
    z, x, y, core = me
    chip = z * 16 + x * 4 + y
    mine = chip * 2 + core
    sp, tp = z * 4 + x, y * 2 + core

    zs = [across(z, k) for k in range(4)]
    xs = [(x + k) % 4 for k in range(4)]
    ys = [(y + k) % 4 for k in range(4)]
    cores = [core, 1 - core]
    tps = [(yt, ct) for yt in ys for ct in cores]
    sps = [(zt, xt) for zt in zs for xt in xs]

    def tok_copy(i):
        kz, kx = step_of(i)
        rows = pl.ds(pl.multiple_of((x + kx) % 4 * ROWS, ROWS), ROWS)
        return pltpu.make_async_copy(tok_hbm.at[across(z, kz), rows], tok.at[i], tok_sem.at[i])

    def in_copy(n, src, dst):
        return pltpu.make_async_copy(src, dst, in_sem.at[n])

    early = [in_copy(0, wk_hbm, wk), in_copy(1, wv_hbm, wv), in_copy(2, gain_hbm, gain)]
    late = [
        in_copy(3, query_hbm, query), in_copy(4, gate_hbm.at[chip], gates.at[core * 64 + chip])
    ]
    tok_copy(0).start()
    for copy in early:
        copy.start()
    tok_copy(1).start()

    barrier = pltpu.get_barrier_semaphore()
    with jax.named_scope("signals"):
        for zt in zs[::-1]:
            for xt in xs[::-1]:
                for yt, ct in tps[::-1]:
                    if zt is not zs[0] or xt is not xs[0] or yt is not ys[0] or ct is not core:
                        pl.semaphore_signal(
                            barrier, inc=1, device_id=device_of((zt, xt, yt, ct)), device_id_type=MESH
                        )

    def send_step(i):
        kz, kx = step_of(i)
        zt, xt = across(z, kz), (x + kx) % 4
        base = zt * 32 + xt * 8
        for j, (yt, ct) in enumerate(tps):

            def one():
                send(
                    made.at[base + yt * 2 + ct], cache.at[mine], wave_sem.at[i], recv_sem.at[0],
                    (zt, xt, yt, ct),
                )

            if j:
                one()
            else:
                pl.when(i != STEPS - 1)(one)

    def await_step(i, n=8):
        await_bytes(made.at[pl.ds(0, n)], wave_sem.at[i])

    def send_gates():
        for zt, xt in sps:
            for yt in ys:
                if zt is not zs[0] or xt is not xs[0] or yt is not ys[0]:
                    send(
                        gate_hbm.at[zt * 16 + xt * 4 + yt], gates.at[core * 64 + chip],
                        send_sem.at[0], recv_sem.at[1], (zt, xt, yt, core),
                    )

    def project(i, n):
        for s in range(n):
            with jax.named_scope("tokwait"):
                tok_copy(i + s).wait()
        with jax.named_scope("norm"):
            for r in range(0, n * ROWS, 16):
                wide = tok[i + r // ROWS, pl.ds(r % ROWS, 16)].astype(jnp.float32)
                mean = jnp.sum(wide * wide, axis=-1, keepdims=True) * (1.0 / wide.shape[-1])
                scale = lax.rsqrt(mean + NORM_FLOOR)
                normed[pl.ds(r, 16)] = (wide * scale * gain[...]).astype(jnp.bfloat16)

        with jax.named_scope("dots"):
            lhs = normed[pl.ds(0, n * ROWS)]
            keys = jnp.dot(lhs, wk[...], preferred_element_type=jnp.float32)
            values = jnp.dot(lhs, wv[...], preferred_element_type=jnp.float32)
            for s in range(n):
                kz, kx = step_of(i + s)
                base = across(z, kz) * 32 + (x + kx) % 4 * 8
                rows = slice(s * ROWS, (s + 1) * ROWS)
                for h in range(4):
                    cols = slice(h * HD, (h + 1) * HD)
                    both = jnp.concatenate([keys[rows, cols], values[rows, cols]], axis=1)
                    both = both.astype(jnp.bfloat16)
                    made[base + 2 * h] = both[:64]
                    made[base + 2 * h + 1] = both[64:]

    mate = (z, x, y, 1 - core)

    with jax.named_scope("inputs"):
        for copy in early:
            copy.wait()
    for i in range(2, 4):
        tok_copy(i).start()
    project(0, 1)
    with jax.named_scope("barrier"):
        pl.semaphore_wait(barrier, 127)
    with jax.named_scope("sendstep"):
        send_step(0)
    with jax.named_scope("sendgates"):
        send_gates()
    for copy in late:
        copy.start()
    for i in range(4, 6):
        tok_copy(i).start()
    project(1, 1)
    send_step(1)

    @pl.loop(2, STEPS, step=2)
    def _(i):
        @pl.when(i < STEPS - 4)
        def _():
            for n in range(4, 6):
                tok_copy(i + n).start()

        project(i, 2)

        @pl.when(i < BURST)
        def _():
            send_step(i)
            send_step(i + 1)

        @pl.when(i == 10)
        def _():
            with jax.named_scope("waitgates"):
                late[1].wait()
                await_bytes(gates.at[pl.ds(0, 63)], recv_sem.at[1])
            held = gates.at[pl.ds(core * 64, 64)]
            send(held, held, send_sem.at[1], recv_sem.at[2], mate)

    late[0].wait()
    with jax.named_scope("selfpiece"):
        cache[mine] = made[mine]

    lane = lax.broadcasted_iota(jnp.int32, (8, 2 * HD), 1)
    lane16 = lax.broadcasted_iota(jnp.int32, (16, 2 * HD), 1)
    for g in range(4):
        wide = query[g].astype(jnp.float32)
        both = jnp.concatenate([wide, jnp.zeros_like(wide)], axis=1)
        for h in range(4):
            padded[g * 4 + h] = both[h * 8 : (h + 1) * 8]

    with jax.named_scope("gatewait"):
        await_bytes(gates.at[pl.ds(0, 64)], recv_sem.at[2])

    with jax.named_scope("attention"):

        @pl.loop(0, 4)
        def _(g):
            for h in range(4):
                for c in range(4):
                    for b in range(2):
                        packed[b, h * 4 + c : h * 4 + c + 1] = gates[b * 64 + g * 16 + c * 4 + h]
            low, high = packed[0], packed[1]
            low_turned, high_turned = (
                jnp.concatenate([t[:, HD:], t[:, :HD]], axis=1) for t in (low, high)
            )
            gate = jnp.where(
                lane16 < HD,
                jnp.where(core == 0, low, low_turned),
                jnp.where(core == 0, high_turned, high),
            )
            for h in range(4):
                q = padded[g * 4 + h].astype(jnp.bfloat16)
                pieces = [
                    made[pl.ds(g * 32 + c * 8 + h * 2, 2)].reshape(ROWS, 2 * HD) for c in range(4)
                ]
                score = jnp.concatenate(
                    [
                        lax.dot_general(q, p, KV, preferred_element_type=jnp.float32) * HD ** (-0.5)
                        - gate[h * 4 + c : h * 4 + c + 1]
                        for c, p in enumerate(pieces)
                    ],
                    axis=1,
                )
                top = jnp.max(score, axis=1, keepdims=True)
                weight = jnp.exp(score - top)
                total = jnp.sum(weight, axis=1, keepdims=True)
                first = weight.astype(jnp.bfloat16).astype(jnp.float32)
                second = (weight - first).astype(jnp.bfloat16).astype(jnp.float32)
                third = weight - first - second
                split = jnp.concatenate([first, second, third], axis=0).astype(jnp.bfloat16)
                out = jnp.dot(
                    split, jnp.concatenate(pieces, axis=0), preferred_element_type=jnp.float32
                )
                out = out[:8] + out[8:16] + out[16:]
                part[g * 4 + h] = jnp.where(lane == 0, top, jnp.where(lane < HD, total, out))

    def send_part():
        for yt, ct in tps[1:]:
            send(
                part.at[pl.ds((yt * 2 + ct) * 2, 2)], part_in.at[pl.ds(tp * 2, 2)],
                send_sem.at[2], recv_sem.at[3], (z, x, yt, ct),
            )

    def send_row():
        with jax.named_scope("wait_part"):
            await_bytes(part_in.at[pl.ds(0, 14)], recv_sem.at[3])
        for n in range(2):
            part_in[tp * 2 + n] = part[tp * 2 + n]
        for n in range(2):
            one = merged([part_in[t * 2 + n] for t in range(8)], lane)
            for j in range(8):
                row[n * 8 + j] = one[j : j + 1]

        for zt, xt in sps[1:]:
            send(
                row.at[zt * 4 + xt], row_in.at[sp], send_sem.at[3], recv_sem.at[4],
                (zt, xt, y, core),
            )

    def send_final():
        with jax.named_scope("wait_row"):
            await_bytes(row_in.at[pl.ds(0, 15)], recv_sem.at[4])
        row_in[sp] = row[sp]
        one = merged([row_in[s] for s in range(16)], lane[:1])
        done = one / one[:, 1:2]
        final[0] = done
        final_in[sp] = done

        for zt, xt in sps[1:]:
            send(
                final.at[0], final_in.at[sp], send_sem.at[4], recv_sem.at[5], (zt, xt, y, core)
            )

    def send_read():
        with jax.named_scope("wait_final"):
            await_bytes(final_in.at[pl.ds(0, 15)], recv_sem.at[5])
        for s in range(16):
            read_in[tp, s] = final_in[s]

        for yt, ct in tps[1:]:
            send(final_in, read_in.at[tp], send_sem.at[5], recv_sem.at[6], (z, x, yt, ct))

    send_part()

    @pl.loop(BURST, STEPS)
    def _(i):
        with jax.named_scope("pace"):
            await_step(i - DEPTH)
        send_step(i)
        pl.when(i == 8)(send_row)
        pl.when(i == 10)(send_final)
        pl.when(i == 12)(send_read)

    with jax.named_scope("wait_read"):
        await_bytes(read_in.at[pl.ds(0, 7)], recv_sem.at[6])
    for t in range(8):
        for s in range(16):
            lined[s : s + 1] = read_in[t, s]
        read[t // 2, t % 2 * 16 : t % 2 * 16 + 16] = lined[...][:, HD:]

    with jax.named_scope("wait_sent"):
        for i in (*range(BURST - DEPTH), *range(STEPS - DEPTH, STEPS)):
            await_step(i, 7 if i == STEPS - 1 else 8)
    await_bytes(gates.at[pl.ds(0, 63)], send_sem.at[0])
    await_bytes(gates.at[pl.ds(0, 64)], send_sem.at[1])
    await_bytes(part_in.at[pl.ds(0, 14)], send_sem.at[2])
    await_bytes(row_in.at[pl.ds(0, 15)], send_sem.at[3])
    await_bytes(final_in.at[pl.ds(0, 15)], send_sem.at[4])
    await_bytes(read_in.at[pl.ds(0, 7)], send_sem.at[5])
    with jax.named_scope("wait_all"):
        await_bytes(cache.at[pl.ds(0, 127)], recv_sem.at[0])


def shards(tokens, norm_gain, w_key, w_value, new_query, cum_gate):
    width = tokens.shape[-1]
    lanes = 2 * HD
    bf16, f32 = jnp.bfloat16, jnp.float32
    kv_cache, first_read = pl.pallas_call(
        kernel,
        out_shape=[
            pltpu.VMEM((128, 64, lanes), bf16),
            pltpu.VMEM(new_query.shape, f32),
        ],
        in_specs=[pl.BlockSpec(memory_space=pl.ANY)] * 6,
        out_specs=[pl.BlockSpec(memory_space=pltpu.VMEM)] * 2,
        scratch_shapes=[
            pltpu.VMEM((STEPS, ROWS, width), bf16),
            pltpu.VMEM((1, width), f32),
            pltpu.VMEM(w_key.shape, bf16),
            pltpu.VMEM(w_value.shape, bf16),
            pltpu.VMEM(new_query.shape, bf16),
            pltpu.VMEM((16, 8, lanes), f32),
            pltpu.VMEM((2 * ROWS, width), bf16),
            pltpu.VMEM((128, 64, lanes), bf16),
            pltpu.VMEM((128, 1, lanes), f32),
            pltpu.VMEM((2, 16, lanes), f32),
            pltpu.VMEM((16, 8, lanes), f32),
            pltpu.VMEM((16, 8, lanes), f32),
            pltpu.VMEM((16, 1, lanes), f32),
            pltpu.VMEM((16, 1, lanes), f32),
            pltpu.VMEM((1, 1, lanes), f32),
            pltpu.VMEM((16, 1, lanes), f32),
            pltpu.VMEM((8, 16, 1, lanes), f32),
            pltpu.VMEM((16, lanes), f32),
            pltpu.SemaphoreType.DMA((STEPS,)),
            pltpu.SemaphoreType.DMA((5,)),
            pltpu.SemaphoreType.DMA((STEPS,)),
            pltpu.SemaphoreType.DMA((6,)),
            pltpu.SemaphoreType.DMA((7,)),
        ],
        compiler_params=pltpu.CompilerParams(collective_id=0, has_side_effects=True),
    )(
        tokens, norm_gain.reshape(1, width), w_key, w_value, new_query,
        cum_gate.reshape(64, 1, lanes),
    )
    return kv_cache.reshape(1, 1, 128 * 64, lanes), first_read


def solution(mesh):
    split = Mesh(mesh.devices.reshape(mesh.shape["gr"], 4, 4, 4, 2), ("gr", *AXES))
    return jax.shard_map(
        shards,
        mesh=split,
        in_specs=(
            P("gr", (*SP, *TP), None), P(), P(), P(), P("gr", None, None), P(("gr", *SP), TP, None)
        ),
        out_specs=(P(("gr", *SP), TP, None, None), P("gr", None, None)),
        check_vma=False,
    )
```

time: 72.9 us -> 64 us (0.88)
  Pallas kernels: 68.2 us -> 61.3 us
  local copies, waits for them, and re-layouts: 3.71 us -> 1.95 us
    pallas_call x1, Pallas kernels: 68.2 us -> 61.3 us  [shards(): pl.pallas_call(kernel, out_shape=[pltpu.VMEM((128, 64, lanes), bf16), plt...]
    unnamed x4 -> x2, local copies, waits for them, and re-layouts: 3.71 us -> 1.95 us
where the time goes in v3:
time: 64 us; the launch traced here: 63.9 us
  Pallas kernels  61.3 us (96%)
  local copies, waits for them, and re-layouts  1.95 us (3%)
  between operations  0.64 us (1%)
    pallas_call x1, Pallas kernels, shards(): pl.pallas_call(kernel, out_shape=[pltpu.VMEM((128, 64, lanes), bf16), plt...  61.3 us
    unnamed x2, local copies, waits for them, and re-layouts  1.95 us

profile of v3, /device:TPU:1, one launch (start us, length us, event | category | flops | bytes accessed | tf_op | source)
XLA Modules:
  0.0 63.9 jit_solution(17198714613946427242)
XLA Ops:
  0.6 61.3 %shard_map.77 = (bf16[128,64,128]{2,1,0:T(8,128)(2,1)S(1)}, f32[4,32,64]{2,1,0:T(8,128)S(1)}) custom-call(bf16[4,512,2048]{2,1,0:T(8,128)(2,1)} %tok_hbm.1, f32[1,2048]{1,0:T(1,128)} %bitcast.5, bf16[2048,256]{1,0:T(8,128)(2,1)} %wk_hbm.1, bf16[2048,256]{1,0:T(8,128)(2,1)} %wv_hbm.1, bf16[4,32,64]{2,1,0:T(8,128)(2,1)} %query_hbm.1, f32[64,1,128]{2,1,0:T(1,128)} %bitcast.4), custom_call_target="tpu_custom_call" | custom-call | tf_op jit(solution)/shard_map/pallas_call | solution.py:337
  61.9 1.3 %copy.10 = bf16[1,1,8192,128]{3,2,1,0:T(8,128)(2,1)} copy(bf16[1,1,8192,128]{3,2,1,0:T(8,128)(2,1)S(1)} %bitcast.3) | data formatting | bytes 4194304
  63.3 0.6 copy.11

commit v4 on v3

--- a/solution.py
+++ b/solution.py
@@ -13,8 +13,8 @@
 NORM_FLOOR = 0.05
 ROWS = 128
 STEPS = 16
-BURST = 8
-DEPTH = 4
+BURST = 6
+FOLLOW = (2, 2, 4, 2)
 KV = (((1,), (1,)), ((), ()))
 
 
@@ -23,9 +23,12 @@
     return ((1 - kz % 2) * z + (kz % 2) * flip + 2 * (kz // 2)) % 4
 
 
-def step_of(i):
+def step_of(z, i):
     j = i % 4
-    return 3 - (j % 2 * 2 + j // 2), (i // 4 + j + 2) % 4
+    one, two = z % 2 * (1 - z // 2), (1 - z % 2) * (z // 2)
+    even = 2 + one + j // 2 * (1 - 2 * one)
+    odd = 1 - two + j // 2 * (2 * two - 1)
+    return even + j % 2 * (odd - even), (i // 4 + j + 2) % 4
 
 
 def device_of(t):
@@ -53,9 +56,9 @@
 
 def kernel(
     tok_hbm, gain_hbm, wk_hbm, wv_hbm, query_hbm, gate_hbm, cache, read,
-    tok, gain, wk, wv, query, padded, normed, made, gates, packed,
+    tok, gain, wk, wv, gate, query, spread, normed, made, gates, packed,
     part, part_in, row, row_in, final, final_in, read_in, lined,
-    tok_sem, in_sem, wave_sem, send_sem, recv_sem,
+    tok_sem, in_sem, wave_sem, send_sem, recv_sem, up_sem,
 ):
     me = tuple(lax.axis_index(a) for a in AXES)
     z, x, y, core = me
@@ -71,60 +74,103 @@
     sps = [(zt, xt) for zt in zs for xt in xs]
 
     def tok_copy(i):
-        kz, kx = step_of(i)
+        kz, kx = step_of(z, i)
         rows = pl.ds(pl.multiple_of((x + kx) % 4 * ROWS, ROWS), ROWS)
-        return pltpu.make_async_copy(tok_hbm.at[across(z, kz), rows], tok.at[i], tok_sem.at[i])
+        return pltpu.make_async_copy(tok_hbm.at[across(z, kz), rows], tok.at[i], tok_sem.at[i % 6])
 
     def in_copy(n, src, dst):
         return pltpu.make_async_copy(src, dst, in_sem.at[n])
 
-    early = [in_copy(0, wk_hbm, wk), in_copy(1, wv_hbm, wv), in_copy(2, gain_hbm, gain)]
-    late = [
-        in_copy(3, query_hbm, query), in_copy(4, gate_hbm.at[chip], gates.at[core * 64 + chip])
+    early = [
+        in_copy(0, wk_hbm, wk), in_copy(1, wv_hbm, wv), in_copy(2, gain_hbm, gain),
+        in_copy(3, gate_hbm, gate),
     ]
+    late = in_copy(4, query_hbm, query)
     tok_copy(0).start()
     for copy in early:
         copy.start()
     tok_copy(1).start()
 
     barrier = pltpu.get_barrier_semaphore()
-    with jax.named_scope("signals"):
-        for zt in zs[::-1]:
-            for xt in xs[::-1]:
-                for yt, ct in tps[::-1]:
-                    if zt is not zs[0] or xt is not xs[0] or yt is not ys[0] or ct is not core:
+    last = len(zs) - 1
+    apart = 1 - lax.axis_index("gr")
+    is_last = z // last * apart
+
+    @pl.when(is_last == 0)
+    def _():
+        with jax.named_scope("signals"):
+            for zt in zs[::-1]:
+                for xt in xs[::-1]:
+                    for yt, ct in tps[::-1]:
+                        if zt is not zs[0] or xt is not xs[0] or yt is not ys[0] or ct is not core:
+                            pl.semaphore_signal(
+                                barrier, inc=1, device_id=device_of((zt, xt, yt, ct)), device_id_type=MESH
+                            )
+
+    def await_entry():
+        pl.semaphore_wait(barrier, 127 - 32 * apart + is_last)
+
+        @pl.when(is_last == 1)
+        def _():
+            for zt in zs[:0:-1]:
+                for xt in xs[::-1]:
+                    for yt, ct in tps[::-1]:
                         pl.semaphore_signal(
-                            barrier, inc=1, device_id=device_of((zt, xt, yt, ct)), device_id_type=MESH
+                            up_sem.at[0], inc=1, device_id=device_of((zt, xt, yt, ct)), device_id_type=MESH
                         )
 
-    def send_step(i):
-        kz, kx = step_of(i)
-        zt, xt = across(z, kz), (x + kx) % 4
-        base = zt * 32 + xt * 8
+    def await_last():
+        @pl.when((1 - is_last) * apart == 1)
+        def _():
+            pl.semaphore_wait(up_sem.at[0], 32)
+
+        @pl.when(z * apart == last - 1)
+        def _():
+            pl.semaphore_signal(
+                up_sem.at[1], inc=1, device_id=device_of((last, x, y, core)), device_id_type=MESH
+            )
+
+        @pl.when(is_last == 1)
+        def _():
+            pl.semaphore_wait(up_sem.at[1], 1)
+
+    def send_steps(i, n):
         for j, (yt, ct) in enumerate(tps):
-
-            def one():
-                send(
-                    made.at[base + yt * 2 + ct], cache.at[mine], wave_sem.at[i], recv_sem.at[0],
-                    (zt, xt, yt, ct),
-                )
-
-            if j:
-                one()
-            else:
-                pl.when(i != STEPS - 1)(one)
-
-    def await_step(i, n=8):
-        await_bytes(made.at[pl.ds(0, n)], wave_sem.at[i])
-
-    def send_gates():
-        for zt, xt in sps:
-            for yt in ys:
-                if zt is not zs[0] or xt is not xs[0] or yt is not ys[0]:
+            for s in range(n):
+                kz, kx = step_of(z, i + s)
+                zt, xt = across(z, kz), (x + kx) % 4
+
+                def one():
                     send(
-                        gate_hbm.at[zt * 16 + xt * 4 + yt], gates.at[core * 64 + chip],
-                        send_sem.at[0], recv_sem.at[1], (zt, xt, yt, core),
+                        made.at[zt * 32 + xt * 8 + yt * 2 + ct], cache.at[mine],
+                        wave_sem.at[(i + s) % BURST], recv_sem.at[0], (zt, xt, yt, ct),
                     )
+
+                if j:
+                    one()
+                else:
+                    pl.when(kz + kx != 0)(one)
+
+    def await_steps(i, n):
+        for s in range(n):
+            sem = wave_sem.at[(i + s) % BURST]
+            kz, kx = step_of(z, i + s)
+            await_bytes(made.at[pl.ds(0, 7)], sem)
+            pl.when(kz + kx != 0)(lambda sem=sem: await_bytes(made.at[pl.ds(0, 1)], sem))
+
+    def send_gates(to_last):
+        for zt in zs:
+
+            def block():
+                for xt in xs:
+                    for yt in ys:
+                        if zt is not zs[0] or xt is not xs[0] or yt is not ys[0]:
+                            send(
+                                gate.at[zt * 16 + xt * 4 + yt], gates.at[core * 64 + chip],
+                                send_sem.at[0], recv_sem.at[1], (zt, xt, yt, core),
+                            )
+
+            pl.when(zt // last * apart == int(to_last))(block)
 
     def project(i, n):
         for s in range(n):
@@ -142,7 +188,7 @@
             keys = jnp.dot(lhs, wk[...], preferred_element_type=jnp.float32)
             values = jnp.dot(lhs, wv[...], preferred_element_type=jnp.float32)
             for s in range(n):
-                kz, kx = step_of(i + s)
+                kz, kx = step_of(z, i + s)
                 base = across(z, kz) * 32 + (x + kx) % 4 * 8
                 rows = slice(s * ROWS, (s + 1) * ROWS)
                 for h in range(4):
@@ -154,6 +200,7 @@
 
     mate = (z, x, y, 1 - core)
 
+    pl.when(is_last == 1)(await_entry)
     with jax.named_scope("inputs"):
         for copy in early:
             copy.wait()
@@ -161,19 +208,26 @@
         tok_copy(i).start()
     project(0, 1)
     with jax.named_scope("barrier"):
-        pl.semaphore_wait(barrier, 127)
-    with jax.named_scope("sendstep"):
-        send_step(0)
+        pl.when(is_last == 0)(await_entry)
     with jax.named_scope("sendgates"):
-        send_gates()
-    for copy in late:
-        copy.start()
+        send_gates(False)
+    gates[core * 64 + chip] = gate[chip]
+    send_steps(0, 1)
+    late.start()
     for i in range(4, 6):
         tok_copy(i).start()
     project(1, 1)
-    send_step(1)
-
-    @pl.loop(2, STEPS, step=2)
+    send_steps(1, 1)
+    project(2, 2)
+    with jax.named_scope("awaitlast"):
+        await_last()
+    with jax.named_scope("sendgates"):
+        send_gates(True)
+    send_steps(2, 2)
+    for i in range(6, 8):
+        tok_copy(i).start()
+
+    @pl.loop(4, STEPS, step=2)
     def _(i):
         @pl.when(i < STEPS - 4)
         def _():
@@ -184,18 +238,16 @@
 
         @pl.when(i < BURST)
         def _():
-            send_step(i)
-            send_step(i + 1)
-
-        @pl.when(i == 10)
+            send_steps(i, 2)
+
+        @pl.when(i == 12)
         def _():
             with jax.named_scope("waitgates"):
-                late[1].wait()
                 await_bytes(gates.at[pl.ds(0, 63)], recv_sem.at[1])
             held = gates.at[pl.ds(core * 64, 64)]
             send(held, held, send_sem.at[1], recv_sem.at[2], mate)
 
-    late[0].wait()
+    late.wait()
     with jax.named_scope("selfpiece"):
         cache[mine] = made[mine]
 
@@ -203,9 +255,9 @@
     lane16 = lax.broadcasted_iota(jnp.int32, (16, 2 * HD), 1)
     for g in range(4):
         wide = query[g].astype(jnp.float32)
-        both = jnp.concatenate([wide, jnp.zeros_like(wide)], axis=1)
+        spread[g] = jnp.zeros(spread.shape[1:], jnp.float32)
         for h in range(4):
-            padded[g * 4 + h] = both[h * 8 : (h + 1) * 8]
+            spread[g, h * 8 : (h + 1) * 8, h * 2 * HD : h * 2 * HD + HD] = wide[h * 8 : (h + 1) * 8]
 
     with jax.named_scope("gatewait"):
         await_bytes(gates.at[pl.ds(0, 64)], recv_sem.at[2])
@@ -222,36 +274,56 @@
             low_turned, high_turned = (
                 jnp.concatenate([t[:, HD:], t[:, :HD]], axis=1) for t in (low, high)
             )
-            gate = jnp.where(
+            bias = jnp.where(
                 lane16 < HD,
                 jnp.where(core == 0, low, low_turned),
                 jnp.where(core == 0, high_turned, high),
             )
+            pairs = jnp.concatenate(
+                [
+                    jnp.concatenate(
+                        [
+                            made[pl.ds(g * 32 + c * 8 + h * 2, 2)].reshape(ROWS, 2 * HD)
+                            for h in range(4)
+                        ],
+                        axis=1,
+                    )
+                    for c in range(4)
+                ],
+                axis=0,
+            )
+            away = jnp.concatenate(
+                [
+                    jnp.broadcast_to(
+                        jnp.concatenate(
+                            [bias[h * 4 + c : h * 4 + c + 1] for c in range(4)], axis=1
+                        ),
+                        (8, 4 * ROWS),
+                    )
+                    for h in range(4)
+                ],
+                axis=0,
+            )
+            score = lax.dot_general(
+                spread[g].astype(jnp.bfloat16), pairs, KV, preferred_element_type=jnp.float32
+            )
+            score = score * HD ** (-0.5) - away
+            top = jnp.max(score, axis=1, keepdims=True)
+            weight = jnp.exp(score - top)
+            total = jnp.sum(weight, axis=1, keepdims=True)
+            first = weight.astype(jnp.bfloat16).astype(jnp.float32)
+            second = (weight - first).astype(jnp.bfloat16).astype(jnp.float32)
+            third = weight - first - second
+            split = jnp.concatenate([first, second, third], axis=0).astype(jnp.bfloat16)
+            out = jnp.dot(split, pairs, preferred_element_type=jnp.float32)
+            out = out[:32] + out[32:64] + out[64:]
             for h in range(4):
-                q = padded[g * 4 + h].astype(jnp.bfloat16)
-                pieces = [
-                    made[pl.ds(g * 32 + c * 8 + h * 2, 2)].reshape(ROWS, 2 * HD) for c in range(4)
-                ]
-                score = jnp.concatenate(
-                    [
-                        lax.dot_general(q, p, KV, preferred_element_type=jnp.float32) * HD ** (-0.5)
-                        - gate[h * 4 + c : h * 4 + c + 1]
-                        for c, p in enumerate(pieces)
-                    ],
-                    axis=1,
+                rows = slice(h * 8, (h + 1) * 8)
+                part[g * 4 + h] = jnp.where(
+                    lane == 0,
+                    top[rows],
+                    jnp.where(lane < HD, total[rows], out[rows, h * 2 * HD : (h + 1) * 2 * HD]),
                 )
-                top = jnp.max(score, axis=1, keepdims=True)
-                weight = jnp.exp(score - top)
-                total = jnp.sum(weight, axis=1, keepdims=True)
-                first = weight.astype(jnp.bfloat16).astype(jnp.float32)
-                second = (weight - first).astype(jnp.bfloat16).astype(jnp.float32)
-                third = weight - first - second
-                split = jnp.concatenate([first, second, third], axis=0).astype(jnp.bfloat16)
-                out = jnp.dot(
-                    split, jnp.concatenate(pieces, axis=0), preferred_element_type=jnp.float32
-                )
-                out = out[:8] + out[8:16] + out[16:]
-                part[g * 4 + h] = jnp.where(lane == 0, top, jnp.where(lane < HD, total, out))
 
     def send_part():
         for yt, ct in tps[1:]:
@@ -299,16 +371,14 @@
         for yt, ct in tps[1:]:
             send(final_in, read_in.at[tp], send_sem.at[5], recv_sem.at[6], (z, x, yt, ct))
 
-    send_part()
-
-    @pl.loop(BURST, STEPS)
-    def _(i):
-        with jax.named_scope("pace"):
-            await_step(i - DEPTH)
-        send_step(i)
-        pl.when(i == 8)(send_row)
-        pl.when(i == 10)(send_final)
-        pl.when(i == 12)(send_read)
+    at = BURST
+    for stage, n in zip((send_part, send_row, send_final, send_read), FOLLOW):
+        stage()
+        if n:
+            with jax.named_scope("pace"):
+                await_steps(at - BURST, n)
+            send_steps(at, n)
+        at += n
 
     with jax.named_scope("wait_read"):
         await_bytes(read_in.at[pl.ds(0, 7)], recv_sem.at[6])
@@ -318,8 +388,7 @@
         read[t // 2, t % 2 * 16 : t % 2 * 16 + 16] = lined[...][:, HD:]
 
     with jax.named_scope("wait_sent"):
-        for i in (*range(BURST - DEPTH), *range(STEPS - DEPTH, STEPS)):
-            await_step(i, 7 if i == STEPS - 1 else 8)
+        await_steps(STEPS - BURST, BURST)
     await_bytes(gates.at[pl.ds(0, 63)], send_sem.at[0])
     await_bytes(gates.at[pl.ds(0, 64)], send_sem.at[1])
     await_bytes(part_in.at[pl.ds(0, 14)], send_sem.at[2])
@@ -330,11 +399,22 @@
         await_bytes(cache.at[pl.ds(0, 127)], recv_sem.at[0])
 
 
+def store_kernel(cache, read, cache_out, read_out, sem):
+    copies = [pltpu.make_async_copy(read, read_out, sem.at[4])] + [
+        pltpu.make_async_copy(cache.at[pl.ds(n * 32, 32)], cache_out.at[pl.ds(n * 32, 32)], sem.at[n])
+        for n in range(4)
+    ]
+    for copy in copies:
+        copy.start()
+    for copy in copies:
+        copy.wait()
+
+
 def shards(tokens, norm_gain, w_key, w_value, new_query, cum_gate):
     width = tokens.shape[-1]
     lanes = 2 * HD
     bf16, f32 = jnp.bfloat16, jnp.float32
-    kv_cache, first_read = pl.pallas_call(
+    cache, read = pl.pallas_call(
         kernel,
         out_shape=[
             pltpu.VMEM((128, 64, lanes), bf16),
@@ -347,8 +427,9 @@
             pltpu.VMEM((1, width), f32),
             pltpu.VMEM(w_key.shape, bf16),
             pltpu.VMEM(w_value.shape, bf16),
+            pltpu.VMEM((64, 1, lanes), f32),
             pltpu.VMEM(new_query.shape, bf16),
-            pltpu.VMEM((16, 8, lanes), f32),
+            pltpu.VMEM((4, 32, 4 * lanes), f32),
             pltpu.VMEM((2 * ROWS, width), bf16),
             pltpu.VMEM((128, 64, lanes), bf16),
             pltpu.VMEM((128, 1, lanes), f32),
@@ -361,17 +442,29 @@
             pltpu.VMEM((16, 1, lanes), f32),
             pltpu.VMEM((8, 16, 1, lanes), f32),
             pltpu.VMEM((16, lanes), f32),
-            pltpu.SemaphoreType.DMA((STEPS,)),
+            pltpu.SemaphoreType.DMA((6,)),
             pltpu.SemaphoreType.DMA((5,)),
-            pltpu.SemaphoreType.DMA((STEPS,)),
+            pltpu.SemaphoreType.DMA((BURST,)),
             pltpu.SemaphoreType.DMA((6,)),
             pltpu.SemaphoreType.DMA((7,)),
+            pltpu.SemaphoreType.REGULAR((2,)),
         ],
         compiler_params=pltpu.CompilerParams(collective_id=0, has_side_effects=True),
     )(
         tokens, norm_gain.reshape(1, width), w_key, w_value, new_query,
         cum_gate.reshape(64, 1, lanes),
     )
+    cache = pltpu.with_memory_space_constraint(cache, pltpu.VMEM)
+    read = pltpu.with_memory_space_constraint(read, pltpu.VMEM)
+    kv_cache, first_read = pl.pallas_call(
+        store_kernel,
+        out_shape=[
+            jax.ShapeDtypeStruct(cache.shape, bf16), jax.ShapeDtypeStruct(read.shape, f32)
+        ],
+        in_specs=[pl.BlockSpec(memory_space=pltpu.VMEM)] * 2,
+        out_specs=[pl.BlockSpec(memory_space=pl.ANY)] * 2,
+        scratch_shapes=[pltpu.SemaphoreType.DMA((5,))],
+    )(cache, read)
     return kv_cache.reshape(1, 1, 128 * 64, lanes), first_read
 
 

time: 64 us -> 59.9 us (0.936)
  Pallas kernels: 61.3 us -> 58.6 us
  local copies, waits for them, and re-layouts: 1.95 us -> 0 us
    pallas_call x1, Pallas kernels: 61.3 us -> 57.2 us  [shards(): pl.pallas_call(kernel, out_shape=[pltpu.VMEM((128, 64, lanes), bf16), plt...]
    unnamed x2 -> x0, local copies, waits for them, and re-layouts: 1.95 us -> none
    pallas_call x0 -> x1, Pallas kernels: none -> 1.38 us  [shards(): pl.pallas_call(store_kernel, out_shape=[jax.ShapeDtypeStruct(cache.shape,...]
where the time goes in v4:
time: 59.9 us; the launch traced here: 59.2 us
  Pallas kernels  58.6 us (98%)
  between operations  0.64 us (1%)
    pallas_call x1, Pallas kernels, shards(): pl.pallas_call(kernel, out_shape=[pltpu.VMEM((128, 64, lanes), bf16), plt...  57.2 us
    pallas_call x1, Pallas kernels, shards(): pl.pallas_call(store_kernel, out_shape=[jax.ShapeDtypeStruct(cache.shape,...  1.38 us

profile of v4, /device:TPU:1, one launch (start us, length us, event | category | flops | bytes accessed | tf_op | source)
XLA Modules:
  0.0 59.2 jit_solution(14848823686301218330)
XLA Ops:
  0.6 57.2 %shard_map.77 = (bf16[128,64,128]{2,1,0:T(8,128)(2,1)S(1)}, f32[4,32,64]{2,1,0:T(8,128)S(1)}) custom-call(bf16[4,512,2048]{2,1,0:T(8,128)(2,1)} %tok_hbm.1, f32[1,2048]{1,0:T(1,128)} %bitcast.4, bf16[2048,256]{1,0:T(8,128)(2,1)} %wk_hbm.1, bf16[2048,256]{1,0:T(8,128)(2,1)} %wv_hbm.1, bf16[4,32,64]{2,1,0:T(8,128)(2,1)} %query_hbm.1, f32[64,1,128]{2,1,0:T(1,128)} %bitcast.3), custom_call_target="tpu_custom_call" | custom-call | tf_op jit(solution)/shard_map/pallas_call | solution.py:417
  57.9 1.4 %shard_map.78 = (bf16[128,64,128]{2,1,0:T(8,128)(2,1)}, f32[4,32,64]{2,1,0:T(8,128)}) custom-call(bf16[128,64,128]{2,1,0:T(8,128)(2,1)S(1)} %get-tuple-element.6.cache, f32[4,32,64]{2,1,0:T(8,128)S(1)} %get-tuple-element.7.read), custom_call_target="tpu_custom_call" | custom-call | tf_op jit(solution)/shard_map/pallas_call | solution.py:459

commit v5 on v4

--- a/solution.py
+++ b/solution.py
@@ -23,9 +23,9 @@
     return ((1 - kz % 2) * z + (kz % 2) * flip + 2 * (kz // 2)) % 4
 
 
-def step_of(z, i):
+def step_of(z, apart, i):
     j = i % 4
-    one, two = z % 2 * (1 - z // 2), (1 - z % 2) * (z // 2)
+    one, two = z % 2 * (1 - z // 2) * apart + 1 - apart, (1 - z % 2) * (z // 2) * apart
     even = 2 + one + j // 2 * (1 - 2 * one)
     odd = 1 - two + j // 2 * (2 * two - 1)
     return even + j % 2 * (odd - even), (i // 4 + j + 2) % 4
@@ -62,6 +62,7 @@
 ):
     me = tuple(lax.axis_index(a) for a in AXES)
     z, x, y, core = me
+    apart = 1 - lax.axis_index("gr")
     chip = z * 16 + x * 4 + y
     mine = chip * 2 + core
     sp, tp = z * 4 + x, y * 2 + core
@@ -74,7 +75,7 @@
     sps = [(zt, xt) for zt in zs for xt in xs]
 
     def tok_copy(i):
-        kz, kx = step_of(z, i)
+        kz, kx = step_of(z, apart, i)
         rows = pl.ds(pl.multiple_of((x + kx) % 4 * ROWS, ROWS), ROWS)
         return pltpu.make_async_copy(tok_hbm.at[across(z, kz), rows], tok.at[i], tok_sem.at[i % 6])
 
@@ -82,7 +83,7 @@
         return pltpu.make_async_copy(src, dst, in_sem.at[n])
 
     early = [
-        in_copy(0, wk_hbm, wk), in_copy(1, wv_hbm, wv), in_copy(2, gain_hbm, gain),
+        in_copy(0, gain_hbm, gain), in_copy(1, wk_hbm, wk), in_copy(2, wv_hbm, wv),
         in_copy(3, gate_hbm, gate),
     ]
     late = in_copy(4, query_hbm, query)
@@ -93,7 +94,6 @@
 
     barrier = pltpu.get_barrier_semaphore()
     last = len(zs) - 1
-    apart = 1 - lax.axis_index("gr")
     is_last = z // last * apart
 
     @pl.when(is_last == 0)
@@ -135,9 +135,10 @@
             pl.semaphore_wait(up_sem.at[1], 1)
 
     def send_steps(i, n):
-        for j, (yt, ct) in enumerate(tps):
+        for j in (4, 5, 2, 3, 6, 7, 0, 1):
+            yt, ct = tps[j]
             for s in range(n):
-                kz, kx = step_of(z, i + s)
+                kz, kx = step_of(z, apart, i + s)
                 zt, xt = across(z, kz), (x + kx) % 4
 
                 def one():
@@ -154,7 +155,7 @@
     def await_steps(i, n):
         for s in range(n):
             sem = wave_sem.at[(i + s) % BURST]
-            kz, kx = step_of(z, i + s)
+            kz, kx = step_of(z, apart, i + s)
             await_bytes(made.at[pl.ds(0, 7)], sem)
             pl.when(kz + kx != 0)(lambda sem=sem: await_bytes(made.at[pl.ds(0, 1)], sem))
 
@@ -172,7 +173,7 @@
 
             pl.when(zt // last * apart == int(to_last))(block)
 
-    def project(i, n):
+    def project(i, n, ahead=()):
         for s in range(n):
             with jax.named_scope("tokwait"):
                 tok_copy(i + s).wait()
@@ -183,12 +184,14 @@
                 scale = lax.rsqrt(mean + NORM_FLOOR)
                 normed[pl.ds(r, 16)] = (wide * scale * gain[...]).astype(jnp.bfloat16)
 
+        for copy in ahead:
+            copy.wait()
         with jax.named_scope("dots"):
             lhs = normed[pl.ds(0, n * ROWS)]
             keys = jnp.dot(lhs, wk[...], preferred_element_type=jnp.float32)
             values = jnp.dot(lhs, wv[...], preferred_element_type=jnp.float32)
             for s in range(n):
-                kz, kx = step_of(z, i + s)
+                kz, kx = step_of(z, apart, i + s)
                 base = across(z, kz) * 32 + (x + kx) % 4 * 8
                 rows = slice(s * ROWS, (s + 1) * ROWS)
                 for h in range(4):
@@ -202,11 +205,10 @@
 
     pl.when(is_last == 1)(await_entry)
     with jax.named_scope("inputs"):
-        for copy in early:
-            copy.wait()
+        early[0].wait()
+    project(0, 1, early[1:])
     for i in range(2, 4):
         tok_copy(i).start()
-    project(0, 1)
     with jax.named_scope("barrier"):
         pl.when(is_last == 0)(await_entry)
     with jax.named_scope("sendgates"):

time: 59.9 us -> 59.4 us (level); the launches traced: 59.2 us -> 59.3 us
  no operation moved by 1% of the time
where the time goes in v5:
time: 59.4 us; the launch traced here: 59.3 us
  Pallas kernels  58.7 us (99%)
  between operations  0.64 us (1%)
    pallas_call x1, Pallas kernels, shards(): pl.pallas_call(kernel, out_shape=[pltpu.VMEM((128, 64, lanes), bf16), plt...  57.3 us
    pallas_call x1, Pallas kernels, shards(): pl.pallas_call(store_kernel, out_shape=[jax.ShapeDtypeStruct(cache.shape,...  1.38 us

profile of v5, /device:TPU:1, one launch (start us, length us, event | category | flops | bytes accessed | tf_op | source)
XLA Modules:
  0.0 59.3 jit_solution(5879138593669579313)
XLA Ops:
  0.6 57.3 %shard_map.77 = (bf16[128,64,128]{2,1,0:T(8,128)(2,1)S(1)}, f32[4,32,64]{2,1,0:T(8,128)S(1)}) custom-call(bf16[4,512,2048]{2,1,0:T(8,128)(2,1)} %tok_hbm.1, f32[1,2048]{1,0:T(1,128)} %bitcast.4, bf16[2048,256]{1,0:T(8,128)(2,1)} %wk_hbm.1, bf16[2048,256]{1,0:T(8,128)(2,1)} %wv_hbm.1, bf16[4,32,64]{2,1,0:T(8,128)(2,1)} %query_hbm.1, f32[64,1,128]{2,1,0:T(1,128)} %bitcast.3), custom_call_target="tpu_custom_call" | custom-call | tf_op jit(solution)/shard_map/pallas_call | solution.py:419
  58.0 1.4 %shard_map.78 = (bf16[128,64,128]{2,1,0:T(8,128)(2,1)}, f32[4,32,64]{2,1,0:T(8,128)}) custom-call(bf16[128,64,128]{2,1,0:T(8,128)(2,1)S(1)} %get-tuple-element.6.cache, f32[4,32,64]{2,1,0:T(8,128)S(1)} %get-tuple-element.7.read), custom_call_target="tpu_custom_call" | custom-call | tf_op jit(solution)/shard_map/pallas_call | solution.py:461

commit v6 on v5

--- a/solution.py
+++ b/solution.py
@@ -14,7 +14,7 @@
 ROWS = 128
 STEPS = 16
 BURST = 6
-FOLLOW = (2, 2, 4, 2)
+FOLLOW = (2, 2, 3, 3)
 KV = (((1,), (1,)), ((), ()))
 
 

time: 59.4 us -> 59.3 us (level)
  no operation moved by 1% of the time
where the time goes in v6:
time: 59.3 us; the launch traced here: 59.2 us
  Pallas kernels  58.5 us (99%)
  between operations  0.64 us (1%)
    pallas_call x1, Pallas kernels, shards(): pl.pallas_call(kernel, out_shape=[pltpu.VMEM((128, 64, lanes), bf16), plt...  57.2 us
    pallas_call x1, Pallas kernels, shards(): pl.pallas_call(store_kernel, out_shape=[jax.ShapeDtypeStruct(cache.shape,...  1.38 us

profile of v6, /device:TPU:1, one launch (start us, length us, event | category | flops | bytes accessed | tf_op | source)
XLA Modules:
  0.0 59.2 jit_solution(12683225047804556956)
XLA Ops:
  0.6 57.2 %shard_map.77 = (bf16[128,64,128]{2,1,0:T(8,128)(2,1)S(1)}, f32[4,32,64]{2,1,0:T(8,128)S(1)}) custom-call(bf16[4,512,2048]{2,1,0:T(8,128)(2,1)} %tok_hbm.1, f32[1,2048]{1,0:T(1,128)} %bitcast.4, bf16[2048,256]{1,0:T(8,128)(2,1)} %wk_hbm.1, bf16[2048,256]{1,0:T(8,128)(2,1)} %wv_hbm.1, bf16[4,32,64]{2,1,0:T(8,128)(2,1)} %query_hbm.1, f32[64,1,128]{2,1,0:T(1,128)} %bitcast.3), custom_call_target="tpu_custom_call" | custom-call | tf_op jit(solution)/shard_map/pallas_call | solution.py:419
  57.8 1.4 %shard_map.78 = (bf16[128,64,128]{2,1,0:T(8,128)(2,1)}, f32[4,32,64]{2,1,0:T(8,128)}) custom-call(bf16[128,64,128]{2,1,0:T(8,128)(2,1)S(1)} %get-tuple-element.6.cache, f32[4,32,64]{2,1,0:T(8,128)S(1)} %get-tuple-element.7.read), custom_call_target="tpu_custom_call" | custom-call | tf_op jit(solution)/shard_map/pallas_call | solution.py:461
